TPU v7x, 128 devices: a whole 4x4x4 slice. The times are simulated.
128 devices in a mesh: sp: 16 (over z, x), tp: 8 (over y, core).
Axes of the slice: x: 4, y: 4, z: 4, core: 2. Of those that a mesh axis runs over, the one named last changes fastest.
Arguments:
- inputs: bfloat16 [8192, 4096], P('sp', 'tp'), may hold values from -6 to 6
- w_value: bfloat16 [4096, 4096], P(None, 'tp'), may hold values from -0.09375 to 0.09375
- w_gate: bfloat16 [4096, 4096], P(None, 'tp'), may hold values from -0.09375 to 0.09375
- taps: bfloat16 [31, 4096], P(None, 'tp'), may hold values from -1 to 1
- ln_gain: float32 [4096], P('tp'), may hold values from 0.1 to 1.9
- w_out: bfloat16 [4096, 4096], P(None, 'tp'), may hold values from -0.09375 to 0.09375
- grad_out: bfloat16 [8192, 4096], P('sp', 'tp'), may hold values from -6 to 6
Outputs:
- grad_input: bfloat16 [8192, 4096], P('sp', 'tp')
- grad_value_w: float32 [4096, 4096], P('sp', 'tp')
- grad_gate_w: float32 [4096, 4096], P('sp', 'tp')
- grad_out_w: float32 [4096, 4096], P('sp', 'tp')
- grad_taps: float32 [31, 4096], P(None, 'tp')
- grad_gain: float32 [4096], P('tp')
All inputs are finite; a program needn't handle non-finite values.
Results may differ from a plain program's by a relative error of at most 0.017.
Values may be sent and summed in bfloat16 or wider, within the bound.
A program may use at most 128 MiB of HBM per device.

v0:
```python
import jax
import jax.numpy as jnp
from jax import lax
from jax.sharding import PartitionSpec as P


def with_halo(cells, sides, width):
    for axis, dim in sides:
        count = lax.axis_size(axis)
        ends = count - 1
        head = lax.slice_in_dim(cells, 0, width, axis=dim)
        tail = lax.slice_in_dim(cells, cells.shape[dim] - width, cells.shape[dim], axis=dim)
        cells = jnp.concatenate(
            [
                lax.ppermute(tail, axis, [(i, (i + 1) % count) for i in range(ends)]),
                cells,
                lax.ppermute(head, axis, [((i + 1) % count, i) for i in range(ends)]),
            ],
            axis=dim,
        )
    return cells


def from_everyone(array, axis):
    copies = jnp.broadcast_to(array, (lax.axis_size(axis), *array.shape))
    return lax.all_to_all(copies, axis, split_axis=0, concat_axis=0, tiled=True)


def over_copies(array, axis):
    return from_everyone(array, axis).sum(axis=0)


def packed_total(arrays, axis):
    ends = [0]
    for a in arrays:
        ends.append(ends[-1] + a.size)
    running = over_copies(jnp.concatenate([a.ravel() for a in arrays]), axis)
    return tuple((running[b:e].reshape(a.shape) for a, b, e in zip(arrays, ends, ends[1:])))


def of_everyone(array, axis):
    everything = from_everyone(array, axis)
    return jnp.sum(everything.astype(jnp.float32), axis=0)


def shifted(value, axis, steps):
    count = lax.axis_size(axis)
    leading, last = (max(0, -steps), min(count, count - steps))
    return lax.ppermute(value, axis, [(source, source + steps) for source in range(leading, last)])


def cut_along(array, dim, count):
    before, after = (array.shape[:dim], array.shape[dim + 1 :])
    return jnp.moveaxis(array.reshape(*before, count, -1, *after), dim, 0)


def summed_on_arrival(array, axis, dim):
    parts = cut_along(array, dim, lax.axis_size(axis))
    arrived = lax.all_to_all(parts, axis, split_axis=0, concat_axis=0, tiled=True)
    return arrived.astype(jnp.float32).sum(axis=0)


def contract_tokens(left, right):
    return lax.dot_general(
        left, right, (((0,), (0,)), ((), ())), preferred_element_type=jnp.float32
    )


def contract_channels(left, right):
    return lax.dot_general(
        left, right, (((1,), (1,)), ((), ())), preferred_element_type=jnp.float32
    )


def local(inputs, w_value, w_gate, taps, ln_gain, w_out, grad_out):
    tok_rows = inputs.shape[0]
    own_width = w_value.shape[1]
    full_width = inputs.shape[1] * lax.axis_size("tp")
    radius = taps.shape[0] // 2
    full_inputs, full_grads = (
        lax.all_gather(inputs, "tp", axis=1, tiled=True),
        lax.all_gather(grad_out, "tp", axis=1, tiled=True),
    )
    pre_value = jnp.dot(full_inputs, w_value, preferred_element_type=jnp.float32)
    pre_gate = jnp.dot(full_inputs, w_gate, preferred_element_type=jnp.float32)
    gate_sigmoid = jax.nn.sigmoid(pre_gate)
    hidden = (pre_value * gate_sigmoid).astype(jnp.bfloat16)
    padded = with_halo(hidden, (("sp", 0),), radius).astype(jnp.float32)
    tap_values = taps.astype(jnp.float32)
    convolved = jnp.zeros((tok_rows, own_width), jnp.float32)
    for offset in range(taps.shape[0]):
        convolved = convolved + tap_values[offset] * padded[offset : offset + tok_rows]
    sum_first, sum_square = packed_total(
        (jnp.sum(convolved, axis=1), jnp.sum(convolved * convolved, axis=1)), "tp"
    )
    mean = (sum_first / full_width)[:, None]
    variance = (sum_square / full_width)[:, None] - mean * mean
    inverse = lax.rsqrt(variance + 1e-06)
    normed = (convolved - mean) * inverse
    scaled = normed * ln_gain
    activated = jax.nn.silu(scaled).astype(jnp.bfloat16)
    grad_act = jnp.dot(full_grads, w_out, preferred_element_type=jnp.float32)
    sig_scaled = jax.nn.sigmoid(scaled)
    grad_scaled = grad_act * sig_scaled * (1.0 + scaled * (1.0 - sig_scaled))
    gain_part = jnp.sum(grad_scaled * normed, axis=0)
    grad_normed = grad_scaled * ln_gain
    first_sum, second_sum = packed_total(
        (jnp.sum(grad_normed, axis=1), jnp.sum(grad_normed * normed, axis=1)), "tp"
    )
    grad_conv = inverse * (
        grad_normed
        - (first_sum / full_width)[:, None]
        - normed * (second_sum / full_width)[:, None]
    )
    tap_rows = []
    for offset in range(taps.shape[0]):
        tap_rows.append(jnp.sum(padded[offset : offset + tok_rows] * grad_conv, axis=0))
    grad_taps, grad_gain = (
        of_everyone(jnp.stack(tap_rows, axis=0).astype(jnp.bfloat16), "sp").astype(jnp.float32),
        of_everyone(gain_part.astype(jnp.bfloat16), "sp").astype(jnp.float32),
    )
    spread = jnp.zeros((tok_rows + 2 * radius, own_width), jnp.float32)
    for offset in range(taps.shape[0]):
        spread = spread + tap_values[offset] * jnp.pad(
            grad_conv, ((offset, 2 * radius - offset), (0, 0))
        )
    from_before = shifted(spread[tok_rows + radius :], "sp", 1)
    from_after = shifted(spread[:radius], "sp", -1)
    grad_hidden = spread[radius : radius + tok_rows]
    grad_hidden = grad_hidden + jnp.pad(from_before, ((0, tok_rows - radius), (0, 0)))
    grad_hidden = grad_hidden + jnp.pad(from_after, ((tok_rows - radius, 0), (0, 0)))
    grad_value = (grad_hidden * gate_sigmoid).astype(jnp.bfloat16)
    grad_gate = (grad_hidden * pre_value * gate_sigmoid * (1.0 - gate_sigmoid)).astype(jnp.bfloat16)
    partial_value = contract_channels(grad_value, w_value) + contract_channels(grad_gate, w_gate)
    grad_input = summed_on_arrival(partial_value.astype(jnp.bfloat16), "tp", 1).astype(jnp.bfloat16)
    both_grads = jnp.concatenate([grad_value, grad_gate], axis=1)
    columns = full_inputs
    stacked = lax.psum_scatter(
        contract_tokens(columns, both_grads).astype(jnp.bfloat16),
        "sp",
        scatter_dimension=0,
        tiled=True,
    ).astype(jnp.float32)
    grad_value_w = stacked[:, :own_width]
    grad_gate_w = stacked[:, own_width:]
    columns = full_grads
    grad_out_w = lax.psum_scatter(
        contract_tokens(columns, activated).astype(jnp.bfloat16),
        "sp",
        scatter_dimension=0,
        tiled=True,
    ).astype(jnp.float32)
    return (grad_input, grad_value_w, grad_gate_w, grad_out_w, grad_taps, grad_gain)


def solution(mesh):
    in_specs = (
        P("sp", "tp"),
        P(None, "tp"),
        P(None, "tp"),
        P(None, "tp"),
        P("tp"),
        P(None, "tp"),
        P("sp", "tp"),
    )
    out_specs = (P("sp", "tp"), P("sp", "tp"), P("sp", "tp"), P("sp", "tp"), P(None, "tp"), P("tp"))
    return jax.shard_map(local, mesh=mesh, in_specs=in_specs, out_specs=out_specs, check_vma=False)
```

profile of v0, /device:TPU:1, one launch (start us, length us, event | category | flops | bytes accessed | tf_op | source)
XLA Modules:
  0.0 264.6 jit_solution(3491135710028727136)
XLA Ops:
  7.2 0.7 all-gather.3.cloned.1.call-update
  7.9 0.7 all-gather.5.cloned.1.call-update
  8.6 0.0 reduce-scatter.5.cloned.1.call-start
  8.7 1.2 fusion.19
  9.9 35.5 %all-gather.3.cloned.1.call-done = bf16[512,4096]{1,0:T(8,128)(2,1)} async-done(((bf16[512,512]{1,0:T(8,128)(2,1)}), bf16[512,4096]{1,0:T(8,128)(2,1)}) %all-gather.3.cloned.1.call-update) | async-done | bytes 4194320 | tf_op jit(solution)/shard_map/all_gather | solution.py:81
  45.4 6.1 %fusion.4 = f32[512,512]{1,0:T(8,128)S(1)} fusion(bf16[512,4096]{1,0:T(8,128)(2,1)} %all-gather.3.cloned.1.call-done, bf16[4096,512]{1,0:T(8,128)(2,1)} %param.9), kind=kOutput, calls=%fused_computation.10 | convolution fusion | flops 2148270080 | bytes 9437184 | tf_op jit(solution)/shard_map/dot_general | solution.py:85
  51.5 3.3 %multiply_convert_fusion.3 = (bf16[512,512]{1,0:T(8,128)(2,1)S(1)}, f32[512,512]{1,0:T(8,128)}) fusion(f32[512,512]{1,0:T(8,128)S(1)} %fusion.4, bf16[512,4096]{1,0:T(8,128)(2,1)S(1)} %copy-done.6, bf16[4096,512]{1,0:T(8,128)(2,1)S(1)} %copy-done), kind=kOutput, calls=%fused_computation.58 | convolution fusion | flops 2148007936 | bytes 11010048 | tf_op jit(solution)/shard_map/dot_general | solution.py:84
  54.8 3.1 %collective-permute-start = (bf16[15,512]{1,0:T(8,128)(2,1)S(1)}, bf16[15,512]{1,0:T(8,128)(2,1)S(1)}, u32[]{:S(2)}, u32[]{:S(2)}) collective-permute-start(bf16[15,512]{1,0:T(8,128)(2,1)S(1)} %get-tuple-element.80), channel_id=1, source_target_pairs={{0,8},{8,16},{16,24},{24,32},{32,40},{40,48},{48,56},{56,64},{64,7... | collective-permute-start | bytes 46088 | tf_op jit(solution)/shard_map/ppermute | solution.py:15
  57.9 1.3 collective-permute-start.1
  59.3 3.5 %collective-permute-done.1 = bf16[15,512]{1,0:T(8,128)(2,1)S(1)} collective-permute-done((bf16[15,512]{1,0:T(8,128)(2,1)S(1)}, bf16[15,512]{1,0:T(8,128)(2,1)S(1)}, u32[]{:S(2)}, u32[]{:S(2)}) %collective-permute-start.1) | collective-permute-done | bytes 15392 | tf_op jit(solution)/shard_map/ppermute | solution.py:17
  62.8 0.2 maximum_convert_fusion
  63.0 5.0 %fusion.15 = (f32[512]{0:T(512)S(1)}, f32[512]{0:T(512)S(1)}, f32[512,512]{1,0:T(8,128)S(1)}) fusion(f32[542,512]{1,0:T(8,128)S(1)} %maximum_convert_fusion, f32[512]{0:T(512)S(1)} %bitcast.116, f32[512]{0:T(512)S(1)} %bitcast.114, f32[512]{0:T(512)S(1)} %bitcast.112, f32[512]{0:T(512)S(1)} %bitcast.110, f32[512]{0:T(512)S(1)} %bitcast.108, ...), kind=kLoop, calls=%fused_computation.75 | loop fusion | flops 16776192 | bytes 33622016 | tf_op jit(solution)/shard_map/reduce_sum | solution.py:94
  68.1 9.1 %all_to_all.28 = f32[8,1,1024]{2,1,0:T(1,128)S(1)} all-to-all(f32[8,1,1024]{2,1,0:T(1,128)S(1)} %broadcast_in_dim.8), channel_id=1, replica_groups=mesh['sp'=16,'tp'=8] {'tp'}, dimensions={0} | all-to-all | bytes 65536 | tf_op jit(solution)/shard_map/all_to_all | solution.py:26
  77.2 2.2 all-gather.5.cloned.1.call-done
  79.4 6.7 %fusion = bf16[4096,512]{0,1:T(8,128)(2,1)} fusion(bf16[512,4096]{1,0:T(8,128)(2,1)} %all-gather.5.cloned.1.call-done, f32[512,512]{1,0:T(8,128)S(1)} %get-tuple-element.73, f32[512]{0:T(512)S(1)} %copy-done.5, f32[512]{0:T(512)S(1)} %get-tuple-element.116, f32[512]{0:T(512)S(1)} %get-tuple-element.115), kind=kOutput, calls=%fused_computation.3 | convolution fusion | flops 2151677952 | bytes 9443328 | tf_op jit(solution)/shard_map/dot_general | solution.py:64
  86.1 0.0 reduce-scatter.3.cloned.1.call-start
  86.2 7.1 %multiply_reduce_fusion = (bf16[512]{0:T(512)(128)(2,1)S(1)}, f32[512]{0:T(512)S(1)}, f32[512]{0:T(512)S(1)}, f32[512,512]{1,0:T(8,128)}) fusion(f32[512,512]{1,0:T(8,128)S(1)} %get-tuple-element.73, f32[512]{0:T(512)S(1)} %get-tuple-element.116, f32[512]{0:T(512)S(1)} %get-tuple-element.115, f32[512]{0:T(512)S(1)} %copy-done.5, ...), kind=kOutput, calls=%fused_computation.17 | convolution fusion | flops 2151938560 | bytes 10497024 | tf_op jit(solution)/shard_map/dot_general | solution.py:102
  93.4 7.7 %all_to_all.29 = f32[8,1,1024]{2,1,0:T(1,128)S(1)} all-to-all(f32[8,1,1024]{2,1,0:T(1,128)S(1)} %broadcast_in_dim.9), channel_id=1, replica_groups=mesh['sp'=16,'tp'=8] {'tp'}, dimensions={0} | all-to-all | bytes 65536 | tf_op jit(solution)/shard_map/all_to_all | solution.py:26
  101.2 4.7 %multiply_reduce_fusion.18 = (bf16[512]{0:T(512)(128)(2,1)S(1)}, bf16[512]{0:T(512)(128)(2,1)S(1)}, bf16[512]{0:T(512)(128)(2,1)S(1)}, bf16[512]{0:T(512)(128)(2...) fusion(f32[542,512]{1,0:T(8,128)S(1)} %maximum_convert_fusion, ...), kind=kLoop, calls=%fused_computation.35 | loop fusion | flops 8644096 | bytes 16800768 | tf_op jit(solution)/shard_map/reduce_sum | solution.py:117
  105.9 5.1 %multiply_add_fusion = f32[542,512]{1,0:T(8,128)S(1)} fusion(f32[512,512]{1,0:T(8,128)S(1)} %get-tuple-element.72, f32[512]{0:T(512)S(1)} %bitcast.117, f32[512]{0:T(512)S(1)} %bitcast.115, f32[512]{0:T(512)S(1)} %bitcast.113, f32[512]{0:T(512)S(1)} %bitcast.111, f32[512]{0:T(512)S(1)} %bitcast.109, f32[512]{0:T(512)S(1)} %bitcast.107, f32[512]{0:T(512)S(1)} %bitcast.105, ...), kind=kLoop, calls=%fused_computation.11 | loop fusion | flops 16927744 | bytes 2222080 | tf_op jit(solution)/shard_map/add | solution.py:124
  111.1 3.1 %collective-permute-start.2 = (f32[15,512]{1,0:T(8,128)S(1)}, f32[15,512]{1,0:T(8,128)S(1)}, u32[]{:S(2)}, u32[]{:S(2)}) collective-permute-start(f32[15,512]{1,0:T(8,128)S(1)} %get-tuple-element.76), channel_id=1, source_target_pairs={{0,8},{8,16},{16,24},{24,32},{32,40},{40,48},{48,56},{56,64},{64,7... | collective-permute-start | bytes 92168 | tf_op jit(solution)/shard_map/ppermute | solution.py:49
  114.2 1.3 collective-permute-start.3
  115.5 4.1 %collective-permute-done.3 = f32[15,512]{1,0:T(8,128)S(1)} collective-permute-done((f32[15,512]{1,0:T(8,128)S(1)}, f32[15,512]{1,0:T(8,128)S(1)}, u32[]{:S(2)}, u32[]{:S(2)}) %collective-permute-start.3) | collective-permute-done | bytes 30752 | tf_op jit(solution)/shard_map/ppermute | solution.py:49
  119.6 0.4 multiply_convert_fusion.2
  120.0 1.8 copy-done.7
  121.8 6.8 %convert_bitcast_fusion = bf16[4096,1024]{0,1:T(8,128)(2,1)} fusion(bf16[512,4096]{1,0:T(8,128)(2,1)S(1)} %copy-done.7, bf16[512,512]{1,0:T(8,128)(2,1)S(1)} %get-tuple-element.75, bf16[512,512]{1,0:T(8,128)(2,1)S(1)} %get-tuple-element.74), kind=kOutput, calls=%fused_computation | convolution fusion | flops 4301258752 | bytes 13631488 | tf_op jit(solution)/shard_map/dot_general | solution.py:64
  128.6 0.5 broadcast.109
  129.1 0.7 reduce.4
  129.9 0.6 reshape.38
  130.5 8.1 %all-to-all-start.4 = ((bf16[16,2,256]{2,1,0:T(2,128)(2,1)}), bf16[16,2,256]{2,1,0:T(2,128)(2,1)S(1)}, u32[]{:S(2)}, u32[]{:S(2)}) async-start(bf16[16,2,256]{2,1,0:T(2,128)(2,1)} %reshape.38), calls=%async_computation.6 | async-start | bytes 32768 | tf_op jit(solution)/shard_map/all_to_all | solution.py:26
  138.6 2.3 multiply_reduce_fusion.1
  141.3 0.2 stack.159
  141.5 7.8 %fusion.21 = f32[512,4096]{1,0:T(8,128)} fusion(bf16[512,512]{1,0:T(8,128)(2,1)S(1)} %get-tuple-element.75, bf16[4096,512]{1,0:T(8,128)(2,1)} %param.9), kind=kOutput, calls=%fused_computation.81 | convolution fusion | flops 2147483648 | bytes 13107200 | tf_op jit(solution)/shard_map/dot_general | solution.py:70
  149.3 0.8 broadcast_in_dim.20
  150.1 6.7 %all-to-all-start.3 = ((bf16[16,31,512]{2,1,0:T(8,128)(2,1)}), bf16[16,31,512]{2,1,0:T(8,128)(2,1)S(1)}, u32[]{:S(2)}, u32[]{:S(2)}) async-start(bf16[16,31,512]{2,1,0:T(8,128)(2,1)} %broadcast_in_dim.20), calls=%async_computation.5 | async-start | bytes 1048576 | tf_op jit(solution)/shard_map/all_to_all | solution.py:26
  156.8 7.1 %add_convert_fusion = bf16[512,4096]{1,0:T(8,128)(2,1)S(1)} fusion(f32[512,4096]{1,0:T(8,128)} %fusion.21, bf16[512,512]{1,0:T(8,128)(2,1)S(1)} %get-tuple-element.74, bf16[4096,512]{1,0:T(8,128)(2,1)} %param.8), kind=kOutput, calls=%fused_computation.1 | convolution fusion | flops 2151677952 | bytes 17301504 | tf_op jit(solution)/shard_map/dot_general | solution.py:70
  163.9 2.3 copy.50
  166.2 1.2 all-to-all-done.3
  167.5 7.0 %all-to-all-start.2 = ((bf16[8,512,512]{2,1,0:T(8,128)(2,1)}), bf16[8,512,512]{2,1,0:T(8,128)(2,1)}, u32[]{:S(2)}, u32[]{:S(2)}) async-start(bf16[8,512,512]{2,1,0:T(8,128)(2,1)} %bitcast.55), calls=%async_computation.2 | async-start | bytes 8388608 | tf_op jit(solution)/shard_map/all_to_all | solution.py:59
  174.5 0.6 convert_reduce_fusion.1
  175.1 1.0 convert_reduce_fusion
  176.1 47.2 %all-to-all-done.2 = bf16[8,512,512]{2,1,0:T(8,128)(2,1)} async-done(((bf16[8,512,512]{2,1,0:T(8,128)(2,1)}), bf16[8,512,512]{2,1,0:T(8,128)(2,1)}, u32[]{:S(2)}, u32[]{:S(2)}) %all-to-all-start.2) | async-done | bytes 4194336 | tf_op jit(solution)/shard_map/all_to_all | solution.py:59
  223.3 3.8 %reduce_sum.378 = bf16[512,512]{1,0:T(8,128)(2,1)} reduce(bf16[8,512,512]{2,1,0:T(8,128)(2,1)} %all-to-all-done.2, bf16[]{:T(256)} %constant.17.clone.1), dimensions={0}, to_apply=%region_6.7 | reduce | flops 1835008 | bytes 4718594 | tf_op jit(solution)/shard_map/reduce_sum | solution.py:60
  227.1 1.9 copy.39
  229.0 26.0 %reduce-scatter.3.cloned.1.call-done = bf16[256,1024]{0,1:T(8,128)(2,1)} async-done(((bf16[4096,1024]{0,1:T(8,128)(2,1)}), bf16[256,1024]{0,1:T(8,128)(2,1)}) %reduce-scatter.3.cloned.1.call-update) | async-done | bytes 524304 | tf_op jit(solution)/shard_map/reduce_scatter | solution.py:138
  255.0 1.1 fusion.17
  256.1 1.0 copy.38
  257.1 1.0 copy.37
  (67 shorter events, 0.5 us)
Async XLA Ops:
  7.2 38.2 %all-gather.3.cloned.1.call-start = ((), (), s32[]{:S(2)}) async-start(), calls=%async_computation.7 | async-start | bytes 4718592 | tf_op jit(solution)/shard_map/all_gather | solution.py:81
  7.9 71.5 %all-gather.5.cloned.1.call-start = ((), (), s32[]{:S(2)}) async-start(), calls=%async_computation.8 | async-start | bytes 4718592 | tf_op jit(solution)/shard_map/all_gather | solution.py:82
  8.6 218.4 %reduce-scatter.5.cloned.1.call-start = ((), (), s32[]{:S(2)}) async-start(), calls=%async_computation.10 | async-start | bytes 4456448 | tf_op jit(solution)/shard_map/reduce_scatter | solution.py:147
  45.4 6.1 %copy-start = (bf16[4096,512]{1,0:T(8,128)(2,1)S(1)}, bf16[4096,512]{1,0:T(8,128)(2,1)}, u32[]{:S(2)}) copy-start(bf16[4096,512]{1,0:T(8,128)(2,1)} %param.8) | copy-start | bytes 12582916
  45.4 6.1 %copy-start.6 = (bf16[512,4096]{1,0:T(8,128)(2,1)S(1)}, bf16[512,4096]{1,0:T(8,128)(2,1)}, u32[]{:S(2)}) copy-start(bf16[512,4096]{1,0:T(8,128)(2,1)} %all-gather.3.cloned.1.call-done) | copy-start | bytes 12582916
  51.5 3.3 %copy-start.1 = (f32[512,512]{1,0:T(8,128)}, f32[512,512]{1,0:T(8,128)S(1)}, u32[]{:S(2)}) copy-start(f32[512,512]{1,0:T(8,128)S(1)} %fusion.4) | copy-start | bytes 3145732
  51.5 7.7 %copy-start.4 = (bf16[31,512]{1,0:T(8,128)(2,1)S(1)}, bf16[31,512]{1,0:T(8,128)(2,1)}, u32[]{:S(2)}) copy-start(bf16[31,512]{1,0:T(8,128)(2,1)} %param.10) | copy-start | bytes 95236
  54.8 4.5 %collective-permute-start = (bf16[15,512]{1,0:T(8,128)(2,1)S(1)}, bf16[15,512]{1,0:T(8,128)(2,1)S(1)}, u32[]{:S(2)}, u32[]{:S(2)}) collective-permute-start(bf16[15,512]{1,0:T(8,128)(2,1)S(1)} %get-tuple-element.80), channel_id=1, source_target_pairs={{0,8},{8,16},{16,24},{24,32},{32,40},{40,48},{48,56},{56,64},{64,7... | collective-permute-start | bytes 46088 | tf_op jit(solution)/shard_map/ppermute | solution.py:15
  57.9 4.9 %collective-permute-start.1 = (bf16[15,512]{1,0:T(8,128)(2,1)S(1)}, bf16[15,512]{1,0:T(8,128)(2,1)S(1)}, u32[]{:S(2)}, u32[]{:S(2)}) collective-permute-start(bf16[15,512]{1,0:T(8,128)(2,1)S(1)} %get-tuple-element.81), channel_id=1, source_target_pairs={{8,0},{16,8},{24,16},{32,24},{40,32},{48,40},{56,48},{64,56},{72,6... | collective-permute-start | bytes 46088 | tf_op jit(solution)/shard_map/ppermute | solution.py:17
  63.0 16.5 %copy-start.5 = (f32[512]{0:T(512)S(1)}, f32[512]{0:T(512)}, u32[]{:S(2)}) copy-start(f32[512]{0:T(512)} %param.11) | copy-start | bytes 6148
  86.1 168.9 %reduce-scatter.3.cloned.1.call-start = ((), (), s32[]{:S(2)}) async-start(), calls=%async_computation.9 | async-start | bytes 8912896 | tf_op jit(solution)/shard_map/reduce_scatter | solution.py:138
  105.9 13.7 %copy-start.2 = (f32[512,512]{1,0:T(8,128)S(1)}, f32[512,512]{1,0:T(8,128)}, u32[]{:S(2)}) copy-start(f32[512,512]{1,0:T(8,128)} %copy-done.1) | copy-start | bytes 3145732
  105.9 13.7 %copy-start.3 = (f32[512,512]{1,0:T(8,128)S(1)}, f32[512,512]{1,0:T(8,128)}, u32[]{:S(2)}) copy-start(f32[512,512]{1,0:T(8,128)} %get-tuple-element.118) | copy-start | bytes 3145732
  111.1 4.4 %collective-permute-start.2 = (f32[15,512]{1,0:T(8,128)S(1)}, f32[15,512]{1,0:T(8,128)S(1)}, u32[]{:S(2)}, u32[]{:S(2)}) collective-permute-start(f32[15,512]{1,0:T(8,128)S(1)} %get-tuple-element.76), channel_id=1, source_target_pairs={{0,8},{8,16},{16,24},{24,32},{32,40},{40,48},{48,56},{56,64},{64,7... | collective-permute-start | bytes 92168 | tf_op jit(solution)/shard_map/ppermute | solution.py:49
  114.2 5.4 %collective-permute-start.3 = (f32[15,512]{1,0:T(8,128)S(1)}, f32[15,512]{1,0:T(8,128)S(1)}, u32[]{:S(2)}, u32[]{:S(2)}) collective-permute-start(f32[15,512]{1,0:T(8,128)S(1)} %get-tuple-element.77), channel_id=1, source_target_pairs={{8,0},{16,8},{24,16},{32,24},{40,32},{48,40},{56,48},{64,56},{72,6... | collective-permute-start | bytes 92168 | tf_op jit(solution)/shard_map/ppermute | solution.py:49
  119.6 2.2 copy-start.7
  130.5 18.8 %all-to-all-start.4 = ((bf16[16,2,256]{2,1,0:T(2,128)(2,1)}), bf16[16,2,256]{2,1,0:T(2,128)(2,1)S(1)}, u32[]{:S(2)}, u32[]{:S(2)}) async-start(bf16[16,2,256]{2,1,0:T(2,128)(2,1)} %reshape.38), calls=%async_computation.6 | async-start | bytes 32768 | tf_op jit(solution)/shard_map/all_to_all | solution.py:26
  150.1 17.4 %all-to-all-start.3 = ((bf16[16,31,512]{2,1,0:T(8,128)(2,1)}), bf16[16,31,512]{2,1,0:T(8,128)(2,1)S(1)}, u32[]{:S(2)}, u32[]{:S(2)}) async-start(bf16[16,31,512]{2,1,0:T(8,128)(2,1)} %broadcast_in_dim.20), calls=%async_computation.5 | async-start | bytes 1048576 | tf_op jit(solution)/shard_map/all_to_all | solution.py:26
  167.5 55.8 %all-to-all-start.2 = ((bf16[8,512,512]{2,1,0:T(8,128)(2,1)}), bf16[8,512,512]{2,1,0:T(8,128)(2,1)}, u32[]{:S(2)}, u32[]{:S(2)}) async-start(bf16[8,512,512]{2,1,0:T(8,128)(2,1)} %bitcast.55), calls=%async_computation.2 | async-start | bytes 8388608 | tf_op jit(solution)/shard_map/all_to_all | solution.py:59
Sparse Core Ops, SparseCore 0:
  9.7 35.6 all-gather.2
  47.1 32.3 all-gather.4
  86.3 77.7 reduce-scatter.4
  167.3 87.6 reduce-scatter.2
where the time goes:
time: 266 us; the launch traced here: 265 us
  waiting for transfers between devices  121 us (45%)
  matrix products  44.8 us (17%)
  starting transfers between devices  30.7 us (12%)
  other arithmetic  24.1 us (9%)
  blocking collectives  16.9 us (6%)
  between operations  14.3 us (5%)
  local copies, waits for them, and re-layouts  12.7 us (5%)
    all_to_all x1, waiting for transfers between devices, summed_on_arrival(): lax.all_to_all(parts, axis, split_axis=0, concat_axis=0, tiled=True)  47.2 us
    all_gather x1, waiting for transfers between devices, local(): lax.all_gather(inputs, 'tp', axis=1, tiled=True)  35.5 us
    reduce_scatter x1, waiting for transfers between devices, local(): lax.psum_scatter(contract_tokens(columns, both_grads).astype(jnp.bfloat16...  26 us
    all_to_all x2, blocking collectives, from_everyone(): return lax.all_to_all(copies, axis, split_axis=0, concat_axis=0, tiled=True)  16.9 us
    dot_general x2, matrix products, contract_channels(): lax.dot_general(left, right, (((1,), (1,)), ((), ())), preferred_element_...  14.9 us
    all_to_all x2, starting transfers between devices, from_everyone(): return lax.all_to_all(copies, axis, split_axis=0, concat_axis=0, tiled=True)  14.8 us
    dot_general x2, matrix products, contract_tokens(): lax.dot_general(left, right, (((0,), (0,)), ((), ())), preferred_element_...  13.4 us
    dot_general x1, matrix products, local(): grad_act = jnp.dot(full_grads, w_out, preferred_element_type=jnp.float32)  7.14 us
  transfers between devices with their start and end apart: 11, of which 7 were waited for; matrix products, arithmetic and copies ran while one was open for 26% of the time, Pallas kernels for 0%

commit v1 on v0

v1 whole, which is shorter than its diff:
```python
import jax
import jax.numpy as jnp
from jax import lax
from jax.experimental import pallas as pl
from jax.experimental.pallas import tpu as pltpu
from jax.sharding import PartitionSpec as P

MESH = pl.DeviceIdType.MESH
F32 = jnp.float32
BF16 = jnp.bfloat16
HI = lax.Precision.HIGHEST
T = 512
C = 512
NB = 8
RAD = 15
TAPS = 31
PAD = 16
COLS = (0, 128, 256, 384)
N_COPIES = 160


def sig(v):
    return 1.0 / (1.0 + jnp.exp(-v))


def dot_nn(a, b):
    return lax.dot_general(a, b, (((1,), (0,)), ((), ())), preferred_element_type=F32)


def dot_nt(a, b):
    return lax.dot_general(a, b, (((1,), (1,)), ((), ())), preferred_element_type=F32)


def dot_tn(a, b):
    return lax.dot_general(a, b, (((0,), (0,)), ((), ())), preferred_element_type=F32)


def kernel(
    x_hbm, g_hbm, wv_hbm, wg_hbm, wo_hbm, taps_ref, gain_ref,
    gi_out, gvw_out, ggw_out, gow_out, taps_out, gain_out,
    X, G, WV, WG, WO, PV, PG, GA, NRM, HID, GC, ACT, GV, GG,
    SA, SQ, MEAN, INV, TF, ST, STR, TP, GP, TG, TGR,
    part, r1, r2, r3, r4, PR, y1, y2, ss, rs, ls,
):
    sp = lax.axis_index("sp")
    tp = lax.axis_index("tp")
    z, x = sp // 4, sp % 4
    y, c = tp // 2, tp % 2

    def at_tp(t):
        return (sp, t)

    def at_y(yy):
        return (sp, (yy % 4) * 2 + c)

    def at_x(xx):
        return (z * 4 + xx % 4, tp)

    def at_z(zz):
        return ((zz % 4) * 4 + x, tp)

    partner = at_tp(y * 2 + (1 - c))

    counter = [0]
    sent = []
    done = []

    def rcopy(src, dst, dev):
        i = counter[0]
        counter[0] += 1
        cp = pltpu.make_async_remote_copy(
            src_ref=src, dst_ref=dst, send_sem=ss.at[i], recv_sem=rs.at[i],
            device_id=dev, device_id_type=MESH,
        )
        cp.start()
        sent.append(cp)
        return cp

    loads = []
    for i, (src, dst) in enumerate(
        ((x_hbm, X.at[tp]), (wv_hbm, WV), (wg_hbm, WG), (g_hbm, G.at[tp]), (wo_hbm, WO))
    ):
        cp = pltpu.make_async_copy(src, dst, ls.at[i])
        cp.start()
        loads.append(cp)

    barrier = pltpu.get_barrier_semaphore()
    peers = [at_tp((tp + d) % 8) for d in range(1, 8)]
    peers += [at_x(x + d) for d in range(1, 4)] + [at_z(z + d) for d in range(1, 4)]
    peers += [((sp + 1) % 16, tp), ((sp + 15) % 16, tp)]
    for dev in peers:
        pl.semaphore_signal(barrier, inc=1, device_id=dev, device_id_type=MESH)
    PV[...] = jnp.zeros((T, C), F32)
    PG[...] = jnp.zeros((T, C), F32)
    GA[...] = jnp.zeros((T, C), F32)
    TF[...] = jnp.zeros((32, C), F32)
    TF[0:TAPS, :] = taps_ref[...].astype(F32)
    pl.semaphore_wait(barrier, len(peers))

    jm = ((y + 3) % 4) * 2 + c
    jp = ((y + 1) % 4) * 2 + c
    jo = ((y + 2) % 4) * 2 + c
    LO, HIH = pl.ds(0, 256), pl.ds(256, 256)

    class Gather:
        def __init__(self, buf):
            self.b = buf

        def start(self):
            b = self.b
            self.h1p = rcopy(b.at[tp, LO], b.at[tp, LO], at_y(y + 1))
            self.h1m = rcopy(b.at[tp, HIH], b.at[tp, HIH], at_y(y + 3))
            self.d0 = rcopy(b.at[tp], b.at[tp], partner)
            self.h2p = rcopy(b.at[tp, HIH], b.at[tp, HIH], at_y(y + 1))
            self.h2m = rcopy(b.at[tp, LO], b.at[tp, LO], at_y(y + 3))

        def first(self):
            b = self.b
            self.h1p.wait_recv()
            self.fp = rcopy(b.at[jm, LO], b.at[jm, LO], at_y(y + 1))
            self.d1p = rcopy(b.at[jm, LO], b.at[jm, LO], partner)
            self.h1m.wait_recv()
            self.fm = rcopy(b.at[jp, HIH], b.at[jp, HIH], at_y(y + 3))
            self.d1m = rcopy(b.at[jp, HIH], b.at[jp, HIH], partner)

        def second(self):
            b = self.b
            self.h2p.wait_recv()
            self.d2p = rcopy(b.at[jm, HIH], b.at[jm, HIH], partner)
            self.h2m.wait_recv()
            self.d2m = rcopy(b.at[jp, LO], b.at[jp, LO], partner)

        def third(self):
            b = self.b
            self.fp.wait_recv()
            self.d3p = rcopy(b.at[jo, LO], b.at[jo, LO], partner)
            self.fm.wait_recv()
            self.d3m = rcopy(b.at[jo, HIH], b.at[jo, HIH], partner)

    def mm(buf, pairs, d_even, d_odd, row_even, row_odd, lo, hi):
        def body(i, _):
            e = i % 2
            par = i // 2
            cc = c + par - 2 * c * par
            j = ((y + d_even + e * (d_odd - d_even)) % 4) * 2 + cc
            row = pl.multiple_of(row_even + e * (row_odd - row_even), 256)
            rows = pl.ds(row, 256)
            a = buf[j, rows, :]
            for w, acc in pairs:
                for n in (0, 256):
                    acc[rows, n:n + 256] += dot_nn(a, w[j, :, n:n + 256])
            return 0

        lax.fori_loop(lo, hi, body, 0)

    gx, gg_ = Gather(X), Gather(G)
    vg = ((WV, PV), (WG, PG))
    wo = ((WO, GA),)
    loads[0].wait()
    gx.start()
    loads[1].wait()
    loads[2].wait()
    mm(X, vg, 0, 0, 0, 256, 0, 2)
    gx.d0.wait_recv()
    mm(X, vg, 0, 0, 0, 256, 2, 4)
    gx.first()
    loads[3].wait()
    gg_.start()
    mm(X, vg, 3, 1, 0, 256, 0, 2)
    gx.d1p.wait_recv()
    gx.d1m.wait_recv()
    mm(X, vg, 3, 1, 0, 256, 2, 4)
    gx.second()
    mm(X, vg, 3, 1, 256, 0, 0, 2)
    gx.d2p.wait_recv()
    gx.d2m.wait_recv()
    mm(X, vg, 3, 1, 256, 0, 2, 4)
    gx.third()
    mm(X, vg, 2, 2, 0, 256, 0, 2)
    gx.d3p.wait_recv()
    gx.d3m.wait_recv()
    mm(X, vg, 2, 2, 0, 256, 2, 4)

    def hidden_body(i, _):
        rows = pl.ds(pl.multiple_of(i * 32, 32), 32)
        out_rows = pl.ds(pl.multiple_of(i * 32 + PAD, 16), 32)
        s = sig(PG[rows, :])
        PG[rows, :] = s
        HID[out_rows, :] = (PV[rows, :] * s).astype(BF16).astype(F32)
        return 0

    lax.fori_loop(0, T // 32, hidden_body, 0)

    following, previous = ((sp + 1) % 16, tp), ((sp + 15) % 16, tp)

    def halo_start(buf):
        up = rcopy(buf.at[pl.ds(T, PAD)], buf.at[pl.ds(0, PAD)], following)
        down = rcopy(buf.at[pl.ds(PAD, PAD)], buf.at[pl.ds(T + PAD, PAD)], previous)
        return up, down

    def halo_finish(buf, pair):
        pair[0].wait_recv()
        pair[1].wait_recv()

        @pl.when(sp == 0)
        def _():
            buf[0:PAD, :] = jnp.zeros((PAD, C), F32)

        @pl.when(sp == 15)
        def _():
            buf[T + PAD:T + 2 * PAD, :] = jnp.zeros((PAD, C), F32)

    halo = halo_start(HID)
    loads[4].wait()
    mm(G, wo, 0, 0, 0, 256, 0, 2)
    gg_.d0.wait_recv()
    mm(G, wo, 0, 0, 0, 256, 2, 4)
    halo_finish(HID, halo)
    gg_.first()

    R = 64

    def conv_tile(src, r0, cs, flip):
        acc = jnp.zeros((R, 128), F32)
        window = src.at[pl.ds(r0, R + 2 * PAD)]
        for o in range(1, TAPS + 1):
            k = TAPS - o if flip else o - 1
            acc = acc + TF[k:k + 1, cs:cs + 128] * window[o:o + R, cs:cs + 128]
        return acc

    def conv_body(i, _):
        r0 = pl.multiple_of(i * R, R)
        rows = pl.ds(r0, R)
        s = jnp.zeros((R, 128), F32)
        q = jnp.zeros((R, 128), F32)
        for cs in COLS:
            v = conv_tile(HID, r0, cs, False)
            NRM[rows, cs:cs + 128] = v
            s = s + v
            q = q + v * v
        SA[rows, :] = s
        SQ[rows, :] = q
        return 0

    lax.fori_loop(0, T // R, conv_body, 0)

    def stats_start(e):
        row = lax.broadcasted_iota(jnp.int32, (8, 128), 0)
        dims = (((1,), (1,)), ((), ()))
        tile = lax.dot_general(
            jnp.where(row == 0, 1.0, 0.0).astype(F32), SA[...], dims, precision=HI, preferred_element_type=F32
        ) + lax.dot_general(
            jnp.where(row == 1, 1.0, 0.0).astype(F32), SQ[...], dims, precision=HI, preferred_element_type=F32
        )
        ST[e] = tile
        STR[e, tp] = tile
        return [rcopy(ST.at[e], STR.at[e, tp], at_tp((tp + d) % 8)) for d in range(1, 8)]

    def stats_finish(e, copies):
        for cp in copies:
            cp.wait_recv()
        row = lax.broadcasted_iota(jnp.int32, (64, 256), 0) & 7
        lane = lax.broadcasted_iota(jnp.int32, (64, 256), 1)
        want = jnp.where(lane < 128, 0, 1)
        pick = jnp.where(row == want, 1.0, 0.0).astype(F32)
        for t in range(0, T, 128):
            block = STR[e, :, :, t:t + 128].reshape(64, 128)
            both = lax.dot_general(
                block, pick, (((0,), (0,)), ((), ())), precision=HI, preferred_element_type=F32
            ) * (1.0 / (NB * C))
            if e == 0:
                mean = both[:, :128]
                MEAN[t:t + 128, :] = mean
                INV[t:t + 128, :] = lax.rsqrt(both[:, 128:] - mean * mean + 1e-06)
            else:
                SA[t:t + 128, :] = both[:, :128]
                SQ[t:t + 128, :] = both[:, 128:]

    stats = stats_start(0)
    mm(G, wo, 3, 1, 0, 256, 0, 2)
    gg_.d1p.wait_recv()
    gg_.d1m.wait_recv()
    mm(G, wo, 3, 1, 0, 256, 2, 4)
    stats_finish(0, stats)

    def norm_body(i, _):
        rows = pl.ds(pl.multiple_of(i * 32, 32), 32)
        m, iv = MEAN[rows, :], INV[rows, :]
        for cs in COLS:
            n = (NRM[rows, cs:cs + 128] - m) * iv
            NRM[rows, cs:cs + 128] = n
            sc = n * gain_ref[0:1, cs:cs + 128]
            ACT[rows, cs:cs + 128] = (sc * sig(sc)).astype(BF16)
        return 0

    lax.fori_loop(0, T // 32, norm_body, 0)

    gg_.second()
    mm(G, wo, 3, 1, 256, 0, 0, 2)
    gg_.d2p.wait_recv()
    gg_.d2m.wait_recv()
    mm(G, wo, 3, 1, 256, 0, 2, 4)
    gg_.third()
    mm(G, wo, 2, 2, 0, 256, 0, 2)
    gg_.d3p.wait_recv()
    gg_.d3m.wait_recv()
    mm(G, wo, 2, 2, 0, 256, 2, 4)

    GP[...] = jnp.zeros((8, C), F32)

    def scaled_body(i, _):
        rows = pl.ds(pl.multiple_of(i * 32, 32), 32)
        s1 = jnp.zeros((32, 128), F32)
        s2 = jnp.zeros((32, 128), F32)
        for cs in COLS:
            n = NRM[rows, cs:cs + 128]
            gain = gain_ref[0:1, cs:cs + 128]
            sc = n * gain
            s = sig(sc)
            gs = GA[rows, cs:cs + 128] * s * (1.0 + sc * (1.0 - s))
            GP[:, cs:cs + 128] += (gs * n).reshape(4, 8, 128).sum(axis=0)
            gn = gs * gain
            GA[rows, cs:cs + 128] = gn
            s1 = s1 + gn
            s2 = s2 + gn * n
        SA[rows, :] = s1
        SQ[rows, :] = s2
        return 0

    lax.fori_loop(0, T // 32, scaled_body, 0)
    stats = stats_start(1)

    at_p = (at_x, at_z)
    at_q = (at_z, at_x)
    me_p = (x, z)
    me_q = (z, x)

    def dw(lhs, units, h, dp):
        p = (me_p[h] + dp) % 4

        def body(q, _):
            zz, xx = (q, p) if h == 0 else (p, q)
            s = zz * 4 + xx
            cols = pl.ds(pl.multiple_of((s % 2) * 256, 256), 256)
            a = lhs[s // 2, :, cols]
            for u, rhs in units:
                part[u, h, p, q] = dot_tn(a, rhs[:, h * 256:h * 256 + 256]).astype(BF16)
            return 0

        lax.fori_loop(0, 4, body, 0)

    class Scatter:
        def __init__(self, u, h):
            self.u, self.h = u, h
            self.p, self.q = me_p[h], me_q[h]

        def blk(self, dp, q0, n=2):
            return part.at[self.u, self.h, (self.p + dp) % 4, pl.ds(q0, n)]

        def s1(self):
            u, h, p = self.u, self.h, self.p
            self.a = rcopy(self.blk(2, 0), r1.at[u, h, 0], at_p[h](p + 1))
            self.b = rcopy(self.blk(2, 2), r1.at[u, h, 1], at_p[h](p + 3))

        def s2i(self):
            u, h, p = self.u, self.h, self.p
            self.c = rcopy(self.blk(1, 2), r2.at[u, h, 0, pl.ds(2, 2)], at_p[h](p + 1))
            self.d = rcopy(self.blk(3, 0), r2.at[u, h, 1, pl.ds(0, 2)], at_p[h](p + 3))

        def add(self, dst_index, rows, sources):
            u, h = self.u, self.h

            def body(i, _):
                rr = pl.ds(pl.multiple_of(rows + i * 32, 32), 32)
                v = part[(u, h) + dst_index + (rr,)].astype(F32)
                for ref, index, off in sources:
                    v = v + ref[index + (pl.ds(pl.multiple_of(off + i * 32, 32), 32),)].astype(F32)
                part[(u, h) + dst_index + (rr,)] = v.astype(BF16)
                return 0

            return body

        def s2d(self):
            u, h, p = self.u, self.h, self.p
            self.a.wait_recv()
            for q in (0, 1):
                lax.fori_loop(0, 8, self.add(((p + 1) % 4, q), 0, [(r1, (u, h, 0, q), 0)]), 0)
            self.e = rcopy(self.blk(1, 0), r2.at[u, h, 0, pl.ds(0, 2)], at_p[h](p + 1))
            self.b.wait_recv()
            for q in (2, 3):
                lax.fori_loop(0, 8, self.add(((p + 3) % 4, q), 0, [(r1, (u, h, 1, q - 2), 0)]), 0)
            self.f = rcopy(self.blk(3, 2), r2.at[u, h, 1, pl.ds(2, 2)], at_p[h](p + 3))

        def p1(self):
            u, h, p, q = self.u, self.h, self.p, self.q
            for cp in (self.c, self.d, self.e, self.f):
                cp.wait_recv()
            for dq in (2, 1, 3, 0):
                qq = (q + dq) % 4
                lax.fori_loop(
                    0, 8, self.add((p, qq), 0, [(r2, (u, h, 0, qq), 0), (r2, (u, h, 1, qq), 0)]), 0
                )
                if dq == 2:
                    src = part.at[u, h, p, qq]
                    self.i = rcopy(src.at[pl.ds(0, 128)], r3.at[u, h, 0], at_q[h](q + 1))
                    self.j = rcopy(src.at[pl.ds(128, 128)], r3.at[u, h, 1], at_q[h](q + 3))

        def p2(self):
            u, h, p, q = self.u, self.h, self.p, self.q
            up, down = (q + 1) % 4, (q + 3) % 4
            self.i.wait_recv()
            lax.fori_loop(0, 4, self.add((p, up), 0, [(r3, (u, h, 0), 0)]), 0)
            self.k = rcopy(part.at[u, h, p, up], r4.at[u, h, 0], at_q[h](q + 1))
            self.j.wait_recv()
            lax.fori_loop(0, 4, self.add((p, down), 128, [(r3, (u, h, 1), 0)]), 0)
            self.l = rcopy(part.at[u, h, p, down], r4.at[u, h, 1], at_q[h](q + 3))

        def finish(self, out):
            u, h, p, q = self.u, self.h, self.p, self.q
            self.k.wait_recv()
            self.l.wait_recv()

            def body(i, _):
                rr = pl.ds(pl.multiple_of(i * 32, 32), 32)
                out[rr, h * 256:h * 256 + 256] = (
                    part[u, h, p, q, rr].astype(F32)
                    + r4[u, h, 0, rr].astype(F32)
                    + r4[u, h, 1, rr].astype(F32)
                )
                return 0

            lax.fori_loop(0, 8, body, 0)

    sc = [[Scatter(u, h) for h in (0, 1)] for u in range(3)]

    def produce(lhs, units):
        for h in (0, 1):
            dw(lhs, units, h, 2)
            for u, _ in units:
                sc[u][h].s1()
        for h in (0, 1):
            dw(lhs, units, h, 1)
            dw(lhs, units, h, 3)
            for u, _ in units:
                sc[u][h].s2i()
        for h in (0, 1):
            dw(lhs, units, h, 0)

    produce(G, [(0, ACT)])
    stats_finish(1, stats)

    def gc_body(i, _):
        rows = pl.ds(pl.multiple_of(i * 32, 32), 32)
        out_rows = pl.ds(pl.multiple_of(i * 32 + PAD, 16), 32)
        f, s, iv = SA[rows, :], SQ[rows, :], INV[rows, :]
        for cs in COLS:
            col = slice(cs, cs + 128)
            GC[out_rows, col] = iv * (GA[rows, col] - f - NRM[rows, col] * s)
        return 0

    lax.fori_loop(0, T // 32, gc_body, 0)
    halo = halo_start(GC)

    for cs in COLS:
        def tap_body(i, accs, cs=cs):
            r0 = pl.multiple_of(i * 8, 8)
            window = HID.at[pl.ds(r0, 8 + 2 * PAD)]
            g = GC[pl.ds(pl.multiple_of(r0 + PAD, 8), 8), cs:cs + 128]
            return tuple(
                a + window[1 + k:9 + k, cs:cs + 128] * g for k, a in enumerate(accs)
            )

        accs = lax.fori_loop(
            0, T // 8, tap_body, tuple(jnp.zeros((8, 128), F32) for _ in range(TAPS))
        )
        for k, a in enumerate(accs):
            TP[k:k + 1, cs:cs + 128] = jnp.sum(a, axis=0, keepdims=True)
    TP[TAPS:TAPS + 1, :] = jnp.sum(GP[...], axis=0, keepdims=True)

    def small_start(e, me, at):
        TGR[e, me] = TG[e]
        return [rcopy(TG.at[e], TGR.at[e, me], at(me + d)) for d in range(1, 4)]

    def small_finish(e, copies):
        for cp in copies:
            cp.wait_recv()
        v = TGR[e, 0].astype(F32)
        for i in range(1, 4):
            v = v + TGR[e, i].astype(F32)
        return v

    TG[0] = TP[...].astype(BF16)
    small = small_start(0, x, at_x)

    for h in (0, 1):
        sc[0][h].s2d()
    halo_finish(GC, halo)

    def back_body(i, _):
        r0 = pl.multiple_of(i * R, R)
        rows = pl.ds(r0, R)
        for cs in COLS:
            col = slice(cs, cs + 128)
            gh = conv_tile(GC, r0, cs, True)
            s = PG[rows, col]
            gv = gh * s
            GV[rows, col] = gv.astype(BF16)
            GG[rows, col] = (gv * PV[rows, col] * (1.0 - s)).astype(BF16)
        return 0

    lax.fori_loop(0, T // R, back_body, 0)

    produce(X, [(1, GV), (2, GG)])

    for h in (0, 1):
        sc[0][h].p1()
    TG[1] = small_finish(0, small).astype(BF16)
    small = small_start(1, z, at_z)

    for cp in (gg_.h1p, gg_.h1m, gg_.d0, gg_.h2p, gg_.h2m, gg_.fp, gg_.fm, gg_.d1p, gg_.d1m,
               gg_.d2p, gg_.d2m, gg_.d3p, gg_.d3m):
        cp.wait_send()
        done.append(id(cp))

    def partial(parity):
        def body(i, _):
            yy = i // 2
            rows = pl.ds(pl.multiple_of((i % 2) * 256, 256), 256)
            j = yy * 2 + parity
            gv, gt = GV[rows, :], GG[rows, :]
            for n in (0, 256):
                G[parity * 4 + yy, rows, n:n + 256] = (
                    dot_nt(gv, WV[j, n:n + 256, :]) + dot_nt(gt, WG[j, n:n + 256, :])
                ).astype(BF16)
            return 0

        lax.fori_loop(0, 8, body, 0)

    partial(1 - c)
    swap = rcopy(G.at[pl.ds((1 - c) * 4, 4)], PR, partner)
    for u in (1, 2):
        for h in (0, 1):
            sc[u][h].s2d()
    partial(c)
    swap.wait_recv()

    def y_add(block, row0, n, sources):
        def body(i, _):
            rr = pl.ds(pl.multiple_of(row0 + i * 32, 32), 32)
            v = G[block, rr].astype(F32)
            for ref, index, off in sources:
                v = v + ref[index + (pl.ds(pl.multiple_of(off + i * 32, 32), 32),)].astype(F32)
            G[block, rr] = v.astype(BF16)
            return 0

        lax.fori_loop(0, n // 32, body, 0)

    base = c * 4
    y2_, yp_, ym_ = (y + 2) % 4, (y + 1) % 4, (y + 3) % 4
    y_add(base + y2_, 0, T, [(PR, (y2_,), 0)])
    ya = rcopy(G.at[base + y2_, LO], y1.at[0], at_y(y + 1))
    yb = rcopy(G.at[base + y2_, HIH], y1.at[1], at_y(y + 3))
    y_add(base + yp_, 0, T, [(PR, (yp_,), 0)])
    yc = rcopy(G.at[base + yp_, HIH], y2.at[0, HIH], at_y(y + 1))
    y_add(base + ym_, 0, T, [(PR, (ym_,), 0)])
    yd = rcopy(G.at[base + ym_, LO], y2.at[1, LO], at_y(y + 3))
    y_add(base + y, 0, T, [(PR, (y,), 0)])

    for h in (0, 1):
        sc[0][h].p2()
    ya.wait_recv()
    y_add(base + yp_, 0, 256, [(y1, (0,), 0)])
    ye = rcopy(G.at[base + yp_, LO], y2.at[0, LO], at_y(y + 1))
    yb.wait_recv()
    y_add(base + ym_, 256, 256, [(y1, (1,), 0)])
    yf = rcopy(G.at[base + ym_, HIH], y2.at[1, HIH], at_y(y + 3))

    for h in (0, 1):
        sc[1][h].p1()
    for h in (0, 1):
        sc[0][h].finish(gow_out)
    total = small_finish(1, small)
    taps_out[...] = total[0:TAPS]
    gain_out[...] = total[TAPS:TAPS + 1]
    for h in (0, 1):
        sc[2][h].p1()
    for h in (0, 1):
        sc[1][h].p2()
    for h in (0, 1):
        sc[2][h].p2()
    for cp in (yc, yd, ye, yf):
        cp.wait_recv()

    def gi_body(i, _):
        rr = pl.ds(pl.multiple_of(i * 32, 32), 32)
        gi_out[rr, :] = (
            G[base + y, rr].astype(F32) + y2[0, rr].astype(F32) + y2[1, rr].astype(F32)
        ).astype(BF16)
        return 0

    lax.fori_loop(0, T // 32, gi_body, 0)
    for h in (0, 1):
        sc[1][h].finish(gvw_out)
    for h in (0, 1):
        sc[2][h].finish(ggw_out)
    for cp in sent:
        if id(cp) not in done:
            cp.wait_send()
    assert counter[0] <= N_COPIES, counter[0]


def local(inputs, w_value, w_gate, taps, ln_gain, w_out, grad_out):
    vm = pltpu.VMEM
    anyspace = pl.BlockSpec(memory_space=pl.ANY)
    in_vmem = pl.BlockSpec(memory_space=pltpu.VMEM)
    shape3 = (NB, C, C)
    gi, gvw, ggw, gow, gt, gg = pl.pallas_call(
        kernel,
        out_shape=(
            jax.ShapeDtypeStruct((T, C), BF16),
            jax.ShapeDtypeStruct((256, C), F32),
            jax.ShapeDtypeStruct((256, C), F32),
            jax.ShapeDtypeStruct((256, C), F32),
            jax.ShapeDtypeStruct((TAPS, C), F32),
            jax.ShapeDtypeStruct((1, C), F32),
        ),
        in_specs=[anyspace] * 5 + [in_vmem] * 2,
        out_specs=(in_vmem,) * 6,
        scratch_shapes=[
            vm((NB, T, C), BF16), vm((NB, T, C), BF16),
            vm(shape3, BF16), vm(shape3, BF16), vm(shape3, BF16),
            vm((T, C), F32), vm((T, C), F32), vm((T, C), F32), vm((T, C), F32),
            vm((T + 2 * PAD, C), F32), vm((T + 2 * PAD, C), F32),
            vm((T, C), BF16), vm((T, C), BF16), vm((T, C), BF16),
            vm((T, 128), F32), vm((T, 128), F32), vm((T, 128), F32), vm((T, 128), F32),
            vm((32, C), F32),
            vm((2, 8, T), F32), vm((2, NB, 8, T), F32),
            vm((32, C), F32), vm((8, C), F32),
            vm((2, 32, C), BF16), vm((2, 4, 32, C), BF16),
            vm((3, 2, 4, 4, 256, 256), BF16),
            vm((3, 2, 2, 2, 256, 256), BF16),
            vm((3, 2, 2, 4, 256, 256), BF16),
            vm((3, 2, 2, 128, 256), BF16),
            vm((3, 2, 2, 256, 256), BF16),
            vm((4, T, C), BF16),
            vm((2, 256, C), BF16), vm((2, T, C), BF16),
            pltpu.SemaphoreType.DMA((N_COPIES,)),
            pltpu.SemaphoreType.DMA((N_COPIES,)),
            pltpu.SemaphoreType.DMA((5,)),
        ],
        compiler_params=pltpu.CompilerParams(
            collective_id=0, has_side_effects=True, vmem_limit_bytes=67043328
        ),
    )(
        inputs, grad_out, w_value.reshape(shape3), w_gate.reshape(shape3), w_out.reshape(shape3),
        taps, ln_gain.reshape(1, C),
    )
    return gi, gvw, ggw, gow, gt, gg.reshape(C)


def solution(mesh):
    in_specs = (
        P("sp", "tp"), P(None, "tp"), P(None, "tp"), P(None, "tp"), P("tp"), P(None, "tp"), P("sp", "tp"),
    )
    out_specs = (P("sp", "tp"), P("sp", "tp"), P("sp", "tp"), P("sp", "tp"), P(None, "tp"), P("tp"))
    return jax.shard_map(local, mesh=mesh, in_specs=in_specs, out_specs=out_specs, check_vma=False)
```

time: 266 us -> 148 us (0.56)
  Pallas kernels: 0 us -> 138 us
  waiting for transfers between devices: 121 us -> 0 us
  matrix products: 44.8 us -> 0 us
  starting transfers between devices: 30.7 us -> 0 us
  other arithmetic: 24.1 us -> 0 us
  blocking collectives: 16.9 us -> 0 us
  between operations: 14.3 us -> 0.66 us
  local copies, waits for them, and re-layouts: 12.7 us -> 8.72 us
    pallas_call x0 -> x1, Pallas kernels: none -> 138 us  [local(): pl.pallas_call(kernel, out_shape=(jax.ShapeDtypeStruct((T, C), BF16), jax...]
    all_to_all x3 -> x0, waiting for transfers between devices: 48.4 us -> none  [the longest x1 47.2 us: summed_on_arrival(): lax.all_to_all(parts, axis, split_axis=0, concat_axis=0, tiled=True)]
    dot_general x7 -> x0, matrix products: 44.8 us -> none  [the longest x2 14.9 us: contract_channels(): lax.dot_general(left, right, (((1,), (1,)), ((), ())), preferred_element_...]
    all_gather x2 -> x0, waiting for transfers between devices: 37.7 us -> none  [the longest x1 35.5 us: local(): lax.all_gather(inputs, 'tp', axis=1, tiled=True)]
    reduce_scatter x2 -> x0, waiting for transfers between devices: 26 us -> none  [the longest x1 26 us: local(): lax.psum_scatter(contract_tokens(columns, both_grads).astype(jnp.bfloat16...]
    all_to_all x3 -> x0, starting transfers between devices: 21.8 us -> none  [the longest x2 14.8 us: from_everyone(): return lax.all_to_all(copies, axis, split_axis=0, concat_axis=0, tiled=True)]
    reduce_sum x8 -> x0, other arithmetic: 17.6 us -> none  [the longest x2 7.08 us: local(): jnp.sum(padded[offset:offset + tok_rows] * grad_conv, axis=0)]
    all_to_all x2 -> x0, blocking collectives: 16.9 us -> none  [from_everyone(): return lax.all_to_all(copies, axis, split_axis=0, concat_axis=0, tiled=True)]
  transfers between devices with their start and end apart: 11 -> 0, of which waited for: 7 -> 0; matrix products, arithmetic and copies ran while one was open for 26% -> 0% of each run, Pallas kernels for 0% -> 0%
where the time goes in v1:
time: 148 us; the launch traced here: 147 us
  Pallas kernels  138 us (93%)
  local copies, waits for them, and re-layouts  8.72 us (6%)
    pallas_call x1, Pallas kernels, local(): pl.pallas_call(kernel, out_shape=(jax.ShapeDtypeStruct((T, C), BF16), jax...  138 us
    unnamed x10, local copies, waits for them, and re-layouts  8.72 us

profile of v1, /device:TPU:1, one launch (start us, length us, event | category | flops | bytes accessed | tf_op | source)
XLA Modules:
  0.0 147.4 jit_solution(9616095858474563730)
XLA Ops:
  0.6 138.0 %shard_map.118 = (bf16[512,512]{1,0:T(8,128)(2,1)}, f32[256,512]{1,0:T(8,128)}, f32[256,512]{1,0:T(8,128)}, f32[256,512]{1,0:T(8,128)}, f32[31,512]{1,0:T(8,128)}, /*index=5*/f32[1,512]{1,0:T(1,128)}) custom-call(bf16[512,512]{1,0:T(8,128)(2,1)} %x_hbm.1, bf16[512,512]{1,0:T(8,128)(2,1)} %g_hbm.1, bf16[8,512,512]{2,1,0:T(8,128)(2,1)} %bitcast.5, ...), custom_call_target="tpu_custom_call" | custom-call | tf_op jit(solution)/shard_map/pallas_call | solution.py:617
  138.7 0.0 copy-start
  138.7 0.0 copy-start.1
  138.7 1.9 %copy.19 = bf16[512,512]{1,0:T(8,128)(2,1)} copy(bf16[512,512]{1,0:T(8,128)(2,1)} %get-tuple-element.24) | data formatting | bytes 1048576
  140.6 1.9 %copy.20 = f32[256,512]{1,0:T(8,128)} copy(f32[256,512]{1,0:T(8,128)} %get-tuple-element.25) | data formatting | bytes 1048576
  142.5 1.9 %copy.21 = f32[256,512]{1,0:T(8,128)} copy(f32[256,512]{1,0:T(8,128)} %get-tuple-element.26) | data formatting | bytes 1048576
  144.3 1.9 %copy.22 = f32[256,512]{1,0:T(8,128)} copy(f32[256,512]{1,0:T(8,128)} %get-tuple-element.27) | data formatting | bytes 1048576
  146.2 0.0 copy-done
  146.2 0.6 copy.23
  146.8 0.0 copy-done.1
  146.8 0.6 copy.24
Async XLA Ops:
  138.7 7.5 %copy-start = (f32[31,512]{1,0:T(8,128)S(1)}, f32[31,512]{1,0:T(8,128)}, u32[]{:S(2)}) copy-start(f32[31,512]{1,0:T(8,128)} %get-tuple-element.28) | copy-start | bytes 190468
  138.7 8.1 %copy-start.1 = (f32[1,512]{1,0:T(1,128)S(1)}, f32[1,512]{1,0:T(1,128)}, u32[]{:S(2)}) copy-start(f32[1,512]{1,0:T(1,128)} %get-tuple-element.17) | copy-start | bytes 6148

commit v2 on v1

--- a/solution.py
+++ b/solution.py
@@ -37,8 +37,8 @@
 
 def kernel(
     x_hbm, g_hbm, wv_hbm, wg_hbm, wo_hbm, taps_ref, gain_ref,
-    gi_out, gvw_out, ggw_out, gow_out, taps_out, gain_out,
-    X, G, WV, WG, WO, PV, PG, GA, NRM, HID, GC, ACT, GV, GG,
+    gi_out, w_out, taps_out,
+    X, G, WV, WG, WO, PV, PG, GA, NRM, HID, GC, ACT, GV, GG, AT, BT,
     SA, SQ, MEAN, INV, TF, ST, STR, TP, GP, TG, TGR,
     part, r1, r2, r3, r4, PR, y1, y2, ss, rs, ls,
 ):
@@ -60,6 +60,15 @@
         return ((zz % 4) * 4 + x, tp)
 
     partner = at_tp(y * 2 + (1 - c))
+
+    scope = [None]
+
+    def mark(name):
+        if scope[0] is not None:
+            scope[0].__exit__(None, None, None)
+        scope[0] = jax.named_scope(name) if name else None
+        if name:
+            scope[0].__enter__()
 
     counter = [0]
     sent = []
@@ -76,6 +85,7 @@
         sent.append(cp)
         return cp
 
+    mark("entry")
     loads = []
     for i, (src, dst) in enumerate(
         ((x_hbm, X.at[tp]), (wv_hbm, WV), (wg_hbm, WG), (g_hbm, G.at[tp]), (wo_hbm, WO))
@@ -156,31 +166,41 @@
     gx, gg_ = Gather(X), Gather(G)
     vg = ((WV, PV), (WG, PG))
     wo = ((WO, GA),)
+    mark("xload")
     loads[0].wait()
     gx.start()
+    mark("wload")
     loads[1].wait()
     loads[2].wait()
+    mark("x0")
     mm(X, vg, 0, 0, 0, 256, 0, 2)
     gx.d0.wait_recv()
     mm(X, vg, 0, 0, 0, 256, 2, 4)
+    mark("x1w")
     gx.first()
     loads[3].wait()
     gg_.start()
+    mark("x1")
     mm(X, vg, 3, 1, 0, 256, 0, 2)
     gx.d1p.wait_recv()
     gx.d1m.wait_recv()
     mm(X, vg, 3, 1, 0, 256, 2, 4)
+    mark("x2w")
     gx.second()
+    mark("x2")
     mm(X, vg, 3, 1, 256, 0, 0, 2)
     gx.d2p.wait_recv()
     gx.d2m.wait_recv()
     mm(X, vg, 3, 1, 256, 0, 2, 4)
+    mark("x3w")
     gx.third()
+    mark("x3")
     mm(X, vg, 2, 2, 0, 256, 0, 2)
     gx.d3p.wait_recv()
     gx.d3m.wait_recv()
     mm(X, vg, 2, 2, 0, 256, 2, 4)
 
+    mark("hidden")
     def hidden_body(i, _):
         rows = pl.ds(pl.multiple_of(i * 32, 32), 32)
         out_rows = pl.ds(pl.multiple_of(i * 32 + PAD, 16), 32)
@@ -210,22 +230,30 @@
         def _():
             buf[T + PAD:T + 2 * PAD, :] = jnp.zeros((PAD, C), F32)
 
+    mark("g0")
     halo = halo_start(HID)
     loads[4].wait()
     mm(G, wo, 0, 0, 0, 256, 0, 2)
     gg_.d0.wait_recv()
     mm(G, wo, 0, 0, 0, 256, 2, 4)
+    mark("halo1w")
     halo_finish(HID, halo)
+    mark("g1w")
     gg_.first()
 
+    mark("conv")
     R = 64
 
     def conv_tile(src, r0, cs, flip):
         acc = jnp.zeros((R, 128), F32)
         window = src.at[pl.ds(r0, R + 2 * PAD)]
-        for o in range(1, TAPS + 1):
-            k = TAPS - o if flip else o - 1
-            acc = acc + TF[k:k + 1, cs:cs + 128] * window[o:o + R, cs:cs + 128]
+        for b in range(8):
+            v = window[b:b + R + 24, cs:cs + 128]
+            for a in range(4):
+                o = 8 * a + b
+                if o:
+                    k = TAPS - o if flip else o - 1
+                    acc = acc + TF[k:k + 1, cs:cs + 128] * v[8 * a:8 * a + R]
         return acc
 
     def conv_body(i, _):
@@ -276,51 +304,50 @@
                 SA[t:t + 128, :] = both[:, :128]
                 SQ[t:t + 128, :] = both[:, 128:]
 
+    mark("stats1")
     stats = stats_start(0)
+    mark("g1")
     mm(G, wo, 3, 1, 0, 256, 0, 2)
     gg_.d1p.wait_recv()
     gg_.d1m.wait_recv()
     mm(G, wo, 3, 1, 0, 256, 2, 4)
-    stats_finish(0, stats)
-
-    def norm_body(i, _):
-        rows = pl.ds(pl.multiple_of(i * 32, 32), 32)
-        m, iv = MEAN[rows, :], INV[rows, :]
-        for cs in COLS:
-            n = (NRM[rows, cs:cs + 128] - m) * iv
-            NRM[rows, cs:cs + 128] = n
-            sc = n * gain_ref[0:1, cs:cs + 128]
-            ACT[rows, cs:cs + 128] = (sc * sig(sc)).astype(BF16)
-        return 0
-
-    lax.fori_loop(0, T // 32, norm_body, 0)
-
+    mark("g2w")
     gg_.second()
+    mark("g2")
     mm(G, wo, 3, 1, 256, 0, 0, 2)
     gg_.d2p.wait_recv()
     gg_.d2m.wait_recv()
     mm(G, wo, 3, 1, 256, 0, 2, 4)
+    mark("g3w")
     gg_.third()
+    mark("g3")
     mm(G, wo, 2, 2, 0, 256, 0, 2)
     gg_.d3p.wait_recv()
     gg_.d3m.wait_recv()
     mm(G, wo, 2, 2, 0, 256, 2, 4)
 
+    mark("stats1w")
+    stats_finish(0, stats)
+    mark("scaled")
     GP[...] = jnp.zeros((8, C), F32)
 
     def scaled_body(i, _):
         rows = pl.ds(pl.multiple_of(i * 32, 32), 32)
+        m, iv = MEAN[rows, :], INV[rows, :]
         s1 = jnp.zeros((32, 128), F32)
         s2 = jnp.zeros((32, 128), F32)
         for cs in COLS:
-            n = NRM[rows, cs:cs + 128]
-            gain = gain_ref[0:1, cs:cs + 128]
+            col = slice(cs, cs + 128)
+            n = (NRM[rows, col] - m) * iv
+            NRM[rows, col] = n
+            gain = gain_ref[0:1, col]
             sc = n * gain
             s = sig(sc)
-            gs = GA[rows, cs:cs + 128] * s * (1.0 + sc * (1.0 - s))
-            GP[:, cs:cs + 128] += (gs * n).reshape(4, 8, 128).sum(axis=0)
+            ACT[rows, col] = (sc * s).astype(BF16)
+            gs = GA[rows, col] * s * (1.0 + sc * (1.0 - s))
+            GP[:, col] += (gs * n).reshape(4, 8, 128).sum(axis=0)
             gn = gs * gain
-            GA[rows, cs:cs + 128] = gn
+            GA[rows, col] = gn
             s1 = s1 + gn
             s2 = s2 + gn * n
         SA[rows, :] = s1
@@ -328,6 +355,7 @@
         return 0
 
     lax.fori_loop(0, T // 32, scaled_body, 0)
+    mark("stats2")
     stats = stats_start(1)
 
     at_p = (at_x, at_z)
@@ -335,16 +363,16 @@
     me_p = (x, z)
     me_q = (z, x)
 
-    def dw(lhs, units, h, dp):
+    def dw(lhs, units, left, h, dp):
         p = (me_p[h] + dp) % 4
 
         def body(q, _):
             zz, xx = (q, p) if h == 0 else (p, q)
             s = zz * 4 + xx
             cols = pl.ds(pl.multiple_of((s % 2) * 256, 256), 256)
-            a = lhs[s // 2, :, cols]
-            for u, rhs in units:
-                part[u, h, p, q] = dot_tn(a, rhs[:, h * 256:h * 256 + 256]).astype(BF16)
+            r = dot_nn(left(h), lhs[s // 2, :, cols]).astype(BF16)
+            for n, u in enumerate(units):
+                part[u, h, p, q] = r[n * 256:n * 256 + 256]
             return 0
 
         lax.fori_loop(0, 4, body, 0)
@@ -415,40 +443,44 @@
             lax.fori_loop(0, 4, self.add((p, down), 128, [(r3, (u, h, 1), 0)]), 0)
             self.l = rcopy(part.at[u, h, p, down], r4.at[u, h, 1], at_q[h](q + 3))
 
-        def finish(self, out):
+        def finish(self):
             u, h, p, q = self.u, self.h, self.p, self.q
             self.k.wait_recv()
             self.l.wait_recv()
-
-            def body(i, _):
-                rr = pl.ds(pl.multiple_of(i * 32, 32), 32)
-                out[rr, h * 256:h * 256 + 256] = (
+            for i in (0, 128):
+                rr = slice(i, i + 128)
+                v = (
                     part[u, h, p, q, rr].astype(F32)
                     + r4[u, h, 0, rr].astype(F32)
                     + r4[u, h, 1, rr].astype(F32)
                 )
-                return 0
-
-            lax.fori_loop(0, 8, body, 0)
+                w_out[u, :, h * 256 + i:h * 256 + i + 128] = v.T.astype(BF16)
 
     sc = [[Scatter(u, h) for h in (0, 1)] for u in range(3)]
 
-    def produce(lhs, units):
+    def produce(lhs, units, left):
         for h in (0, 1):
-            dw(lhs, units, h, 2)
-            for u, _ in units:
+            dw(lhs, units, left, h, 2)
+            for u in units:
                 sc[u][h].s1()
         for h in (0, 1):
-            dw(lhs, units, h, 1)
-            dw(lhs, units, h, 3)
-            for u, _ in units:
+            dw(lhs, units, left, h, 1)
+            dw(lhs, units, left, h, 3)
+            for u in units:
                 sc[u][h].s2i()
         for h in (0, 1):
-            dw(lhs, units, h, 0)
-
-    produce(G, [(0, ACT)])
+            dw(lhs, units, left, h, 0)
+
+    def flip(src, dst, k):
+        for cs in COLS:
+            dst[cs // 256, k + cs % 256:k + cs % 256 + 128, :] = src[:, cs:cs + 128].T
+
+    flip(ACT, AT, 0)
+    produce(G, [0], lambda h: AT[h])
+    mark("stats2w")
     stats_finish(1, stats)
 
+    mark("gc")
     def gc_body(i, _):
         rows = pl.ds(pl.multiple_of(i * 32, 32), 32)
         out_rows = pl.ds(pl.multiple_of(i * 32 + PAD, 16), 32)
@@ -461,17 +493,24 @@
     lax.fori_loop(0, T // 32, gc_body, 0)
     halo = halo_start(GC)
 
+    mark("taps")
     for cs in COLS:
         def tap_body(i, accs, cs=cs):
-            r0 = pl.multiple_of(i * 8, 8)
-            window = HID.at[pl.ds(r0, 8 + 2 * PAD)]
-            g = GC[pl.ds(pl.multiple_of(r0 + PAD, 8), 8), cs:cs + 128]
-            return tuple(
-                a + window[1 + k:9 + k, cs:cs + 128] * g for k, a in enumerate(accs)
-            )
+            r0 = pl.multiple_of(i * 32, 32)
+            window = HID.at[pl.ds(r0, 32 + 2 * PAD)]
+            g = GC[pl.ds(pl.multiple_of(r0 + PAD, 16), 32), cs:cs + 128]
+            accs = list(accs)
+            for b in range(8):
+                v = window[b:b + 56, cs:cs + 128]
+                for a in range(4):
+                    o = 8 * a + b
+                    if o:
+                        prod = v[8 * a:8 * a + 32] * g
+                        accs[o - 1] = accs[o - 1] + prod.reshape(4, 8, 128).sum(axis=0)
+            return tuple(accs)
 
         accs = lax.fori_loop(
-            0, T // 8, tap_body, tuple(jnp.zeros((8, 128), F32) for _ in range(TAPS))
+            0, T // 32, tap_body, tuple(jnp.zeros((8, 128), F32) for _ in range(TAPS))
         )
         for k, a in enumerate(accs):
             TP[k:k + 1, cs:cs + 128] = jnp.sum(a, axis=0, keepdims=True)
@@ -489,13 +528,16 @@
             v = v + TGR[e, i].astype(F32)
         return v
 
+    mark("ow_s2d")
     TG[0] = TP[...].astype(BF16)
     small = small_start(0, x, at_x)
 
     for h in (0, 1):
         sc[0][h].s2d()
+    mark("halo2w")
     halo_finish(GC, halo)
 
+    mark("back")
     def back_body(i, _):
         r0 = pl.multiple_of(i * R, R)
         rows = pl.ds(r0, R)
@@ -510,13 +552,18 @@
 
     lax.fori_loop(0, T // R, back_body, 0)
 
-    produce(X, [(1, GV), (2, GG)])
-
+    mark("vg_dw")
+    flip(GV, BT, 0)
+    flip(GG, BT, 256)
+    produce(X, [1, 2], lambda h: BT[h])
+
+    mark("ow_p1")
     for h in (0, 1):
         sc[0][h].p1()
     TG[1] = small_finish(0, small).astype(BF16)
     small = small_start(1, z, at_z)
 
+    mark("partial1")
     for cp in (gg_.h1p, gg_.h1m, gg_.d0, gg_.h2p, gg_.h2m, gg_.fp, gg_.fm, gg_.d1p, gg_.d1m,
                gg_.d2p, gg_.d2m, gg_.d3p, gg_.d3m):
         cp.wait_send()
@@ -538,10 +585,13 @@
 
     partial(1 - c)
     swap = rcopy(G.at[pl.ds((1 - c) * 4, 4)], PR, partner)
+    mark("vg_s2d")
     for u in (1, 2):
         for h in (0, 1):
             sc[u][h].s2d()
+    mark("partial2")
     partial(c)
+    mark("yadd")
     swap.wait_recv()
 
     def y_add(block, row0, n, sources):
@@ -566,8 +616,10 @@
     yd = rcopy(G.at[base + ym_, LO], y2.at[1, LO], at_y(y + 3))
     y_add(base + y, 0, T, [(PR, (y,), 0)])
 
+    mark("ow_p2")
     for h in (0, 1):
         sc[0][h].p2()
+    mark("y_s2")
     ya.wait_recv()
     y_add(base + yp_, 0, 256, [(y1, (0,), 0)])
     ye = rcopy(G.at[base + yp_, LO], y2.at[0, LO], at_y(y + 1))
@@ -575,19 +627,24 @@
     y_add(base + ym_, 256, 256, [(y1, (1,), 0)])
     yf = rcopy(G.at[base + ym_, HIH], y2.at[1, HIH], at_y(y + 3))
 
+    mark("v_p1")
     for h in (0, 1):
         sc[1][h].p1()
-    for h in (0, 1):
-        sc[0][h].finish(gow_out)
+    mark("ow_fin")
+    for h in (0, 1):
+        sc[0][h].finish()
     total = small_finish(1, small)
-    taps_out[...] = total[0:TAPS]
-    gain_out[...] = total[TAPS:TAPS + 1]
+    taps_out[...] = total
+    mark("g_p1")
     for h in (0, 1):
         sc[2][h].p1()
+    mark("v_p2")
     for h in (0, 1):
         sc[1][h].p2()
+    mark("g_p2")
     for h in (0, 1):
         sc[2][h].p2()
+    mark("y_fin")
     for cp in (yc, yd, ye, yf):
         cp.wait_recv()
 
@@ -599,14 +656,42 @@
         return 0
 
     lax.fori_loop(0, T // 32, gi_body, 0)
-    for h in (0, 1):
-        sc[1][h].finish(gvw_out)
-    for h in (0, 1):
-        sc[2][h].finish(ggw_out)
+    mark("fin")
+    for h in (0, 1):
+        sc[1][h].finish()
+    for h in (0, 1):
+        sc[2][h].finish()
+    mark("sends")
     for cp in sent:
         if id(cp) not in done:
             cp.wait_send()
+    mark(None)
     assert counter[0] <= N_COPIES, counter[0]
+
+
+def unpack(gi_in, w_in, small_in, gi, gvw, ggw, gow, gt, gg, b_gi, b_in, b_out, b_small, si, so):
+    reads = [
+        pltpu.make_async_copy(w_in.at[u], b_in.at[u], si.at[u]) for u in range(3)
+    ] + [
+        pltpu.make_async_copy(gi_in, b_gi, si.at[3]),
+        pltpu.make_async_copy(small_in, b_small, si.at[4]),
+    ]
+    for cp in reads:
+        cp.start()
+    writes = []
+    for u, dst in enumerate((gow, gvw, ggw)):
+        reads[u].wait()
+        b_out[u] = b_in[u].astype(F32)
+        writes.append(pltpu.make_async_copy(b_out.at[u], dst, so.at[u]))
+        writes[-1].start()
+    reads[3].wait()
+    writes.append(pltpu.make_async_copy(b_gi, gi, so.at[3]))
+    writes[-1].start()
+    reads[4].wait()
+    gt[...] = b_small[0:TAPS]
+    gg[...] = b_small[TAPS:TAPS + 1]
+    for cp in writes:
+        cp.wait()
 
 
 def local(inputs, w_value, w_gate, taps, ln_gain, w_out, grad_out):
@@ -614,24 +699,22 @@
     anyspace = pl.BlockSpec(memory_space=pl.ANY)
     in_vmem = pl.BlockSpec(memory_space=pltpu.VMEM)
     shape3 = (NB, C, C)
-    gi, gvw, ggw, gow, gt, gg = pl.pallas_call(
+    gi, w3, small = pl.pallas_call(
         kernel,
         out_shape=(
             jax.ShapeDtypeStruct((T, C), BF16),
-            jax.ShapeDtypeStruct((256, C), F32),
-            jax.ShapeDtypeStruct((256, C), F32),
-            jax.ShapeDtypeStruct((256, C), F32),
-            jax.ShapeDtypeStruct((TAPS, C), F32),
-            jax.ShapeDtypeStruct((1, C), F32),
+            jax.ShapeDtypeStruct((3, 256, C), BF16),
+            jax.ShapeDtypeStruct((32, C), F32),
         ),
         in_specs=[anyspace] * 5 + [in_vmem] * 2,
-        out_specs=(in_vmem,) * 6,
+        out_specs=(in_vmem,) * 3,
         scratch_shapes=[
             vm((NB, T, C), BF16), vm((NB, T, C), BF16),
             vm(shape3, BF16), vm(shape3, BF16), vm(shape3, BF16),
             vm((T, C), F32), vm((T, C), F32), vm((T, C), F32), vm((T, C), F32),
             vm((T + 2 * PAD, C), F32), vm((T + 2 * PAD, C), F32),
             vm((T, C), BF16), vm((T, C), BF16), vm((T, C), BF16),
+            vm((2, 256, T), BF16), vm((2, 512, T), BF16),
             vm((T, 128), F32), vm((T, 128), F32), vm((T, 128), F32), vm((T, 128), F32),
             vm((32, C), F32),
             vm((2, 8, T), F32), vm((2, NB, 8, T), F32),
@@ -655,6 +738,23 @@
         inputs, grad_out, w_value.reshape(shape3), w_gate.reshape(shape3), w_out.reshape(shape3),
         taps, ln_gain.reshape(1, C),
     )
+    gi, gvw, ggw, gow, gt, gg = pl.pallas_call(
+        unpack,
+        out_shape=(
+            jax.ShapeDtypeStruct((T, C), BF16),
+            jax.ShapeDtypeStruct((256, C), F32),
+            jax.ShapeDtypeStruct((256, C), F32),
+            jax.ShapeDtypeStruct((256, C), F32),
+            jax.ShapeDtypeStruct((TAPS, C), F32),
+            jax.ShapeDtypeStruct((1, C), F32),
+        ),
+        in_specs=[anyspace] * 3,
+        out_specs=(anyspace,) * 4 + (in_vmem,) * 2,
+        scratch_shapes=[
+            vm((T, C), BF16), vm((3, 256, C), BF16), vm((3, 256, C), F32), vm((32, C), F32),
+            pltpu.SemaphoreType.DMA((5,)), pltpu.SemaphoreType.DMA((4,)),
+        ],
+    )(gi, w3, small)
     return gi, gvw, ggw, gow, gt, gg.reshape(C)
 
 

time: 148 us -> 134 us (0.905)
  local copies, waits for them, and re-layouts: 8.72 us -> 0 us
  Pallas kernels: 138 us -> 133 us
    unnamed x10 -> x0, local copies, waits for them, and re-layouts: 8.72 us -> none
    pallas_call x1, Pallas kernels: 138 us -> 130 us  [local(): pl.pallas_call(kernel, out_shape=(jax.ShapeDtypeStruct((T, C), BF16), jax...]
    pallas_call x0 -> x1, Pallas kernels: none -> 3.01 us  [local(): pl.pallas_call(unpack, out_shape=(jax.ShapeDtypeStruct((T, C), BF16), jax...]
where the time goes in v2:
time: 134 us
  Pallas kernels  133 us (99%)
    pallas_call x1, Pallas kernels, local(): pl.pallas_call(kernel, out_shape=(jax.ShapeDtypeStruct((T, C), BF16), jax...  130 us
    pallas_call x1, Pallas kernels, local(): pl.pallas_call(unpack, out_shape=(jax.ShapeDtypeStruct((T, C), BF16), jax...  3.01 us

profile of v2, /device:TPU:1, one launch (start us, length us, event | category | flops | bytes accessed | tf_op | source)
XLA Modules:
  0.0 133.8 jit_solution(4800683337055648224)
XLA Ops:
  0.6 129.9 %shard_map.118 = (bf16[512,512]{1,0:T(8,128)(2,1)}, bf16[3,256,512]{2,1,0:T(8,128)(2,1)}, f32[32,512]{1,0:T(8,128)}) custom-call(bf16[512,512]{1,0:T(8,128)(2,1)} %x_hbm.1, bf16[512,512]{1,0:T(8,128)(2,1)} %g_hbm.1, bf16[8,512,512]{2,1,0:T(8,128)(2,1)} %bitcast.5, bf16[8,512,512]{2,1,0:T(8,128)(2,1)} %bitcast.6, bf16[8,512,512]{2,1,0:T(8,128)(2,1)} %bitcast.7, ...), custom_call_target="tpu_custom_call" | custom-call | tf_op jit(solution)/shard_map/pallas_call | solution.py:702
  130.6 3.0 %shard_map.119 = (bf16[512,512]{1,0:T(8,128)(2,1)}, f32[256,512]{1,0:T(8,128)}, f32[256,512]{1,0:T(8,128)}, f32[256,512]{1,0:T(8,128)}, f32[31,512]{1,0:T(8,128)}, /*index=5*/f32[1,512]{1,0:T(1,128)}) custom-call(bf16[512,512]{1,0:T(8,128)(2,1)} %get-tuple-element.15.gi_in, bf16[3,256,512]{2,1,0:T(8,128)(2,1)} %get-tuple-element.16.w_in, ...), custom_call_target="tpu_custom_call" | custom-call | tf_op jit(solution)/shard_map/pallas_call | solution.py:741

commit v3 on v2

--- a/solution.py
+++ b/solution.py
@@ -37,10 +37,10 @@
 
 def kernel(
     x_hbm, g_hbm, wv_hbm, wg_hbm, wo_hbm, taps_ref, gain_ref,
-    gi_out, w_out, taps_out,
+    gi_out, w_out, small_out,
     X, G, WV, WG, WO, PV, PG, GA, NRM, HID, GC, ACT, GV, GG, AT, BT,
     SA, SQ, MEAN, INV, TF, ST, STR, TP, GP, TG, TGR,
-    part, r1, r2, r3, r4, PR, y1, y2, ss, rs, ls,
+    part, r1, r2, r3, r4, XA, XB, BTR, VACC, VP, r3v, r4v, PR, y1, y2, ss, rs, ls,
 ):
     sp = lax.axis_index("sp")
     tp = lax.axis_index("tp")
@@ -163,6 +163,41 @@
 
         lax.fori_loop(lo, hi, body, 0)
 
+    toks = pl.ds(pl.multiple_of(c * 256, 256), 256)
+    ex_a = []
+    b0 = counter[0]
+    counter[0] += 3
+
+    def ex_b(d, yy):
+        return pltpu.make_async_remote_copy(
+            src_ref=X.at[pl.ds(2 * yy, 2), toks], dst_ref=XB.at[d - 1, :, toks],
+            send_sem=ss.at[b0 + d - 1], recv_sem=rs.at[b0 + d - 1],
+            device_id=at_z(z + d), device_id_type=MESH,
+        )
+
+    def exchange(yy):
+        yy = yy % 4
+        for d in (1, 3, 2):
+            t = (x + d) % 4
+            cols = pl.ds(pl.multiple_of((t % 2) * 256, 256), 256)
+            ex_a.append((d, rcopy(X.at[yy * 2 + t // 2, toks, cols], XA.at[d - 1, yy, toks], at_x(t))))
+
+        @pl.when(yy != z)
+        def _():
+            ex_b((yy + 4 - z) % 4, yy).start()
+
+    def exchange_relay():
+        out = []
+        for d in (1, 3, 2):
+            for dd, cp in ex_a:
+                if dd == d:
+                    cp.wait_recv()
+            out.append(rcopy(XA.at[d - 1, :, toks], XA.at[d - 1, :, toks], partner))
+        for d in (1, 3, 2):
+            ex_b(d, y).wait_recv()
+            out.append(rcopy(XB.at[d - 1, :, toks], XB.at[d - 1, :, toks], partner))
+        return out
+
     gx, gg_ = Gather(X), Gather(G)
     vg = ((WV, PV), (WG, PG))
     wo = ((WO, GA),)
@@ -175,6 +210,7 @@
     mark("x0")
     mm(X, vg, 0, 0, 0, 256, 0, 2)
     gx.d0.wait_recv()
+    exchange(y)
     mm(X, vg, 0, 0, 0, 256, 2, 4)
     mark("x1w")
     gx.first()
@@ -184,6 +220,7 @@
     mm(X, vg, 3, 1, 0, 256, 0, 2)
     gx.d1p.wait_recv()
     gx.d1m.wait_recv()
+    exchange(y + 3 + 2 * c)
     mm(X, vg, 3, 1, 0, 256, 2, 4)
     mark("x2w")
     gx.second()
@@ -204,9 +241,11 @@
     def hidden_body(i, _):
         rows = pl.ds(pl.multiple_of(i * 32, 32), 32)
         out_rows = pl.ds(pl.multiple_of(i * 32 + PAD, 16), 32)
-        s = sig(PG[rows, :])
-        PG[rows, :] = s
-        HID[out_rows, :] = (PV[rows, :] * s).astype(BF16).astype(F32)
+        for n, cs in enumerate(COLS):
+            col = slice(cs, cs + 128)
+            s = sig(PG[rows, col])
+            PG[rows, col] = s
+            HID[n, out_rows, :] = (PV[rows, col] * s).astype(BF16).astype(F32)
         return 0
 
     lax.fori_loop(0, T // 32, hidden_body, 0)
@@ -214,8 +253,8 @@
     following, previous = ((sp + 1) % 16, tp), ((sp + 15) % 16, tp)
 
     def halo_start(buf):
-        up = rcopy(buf.at[pl.ds(T, PAD)], buf.at[pl.ds(0, PAD)], following)
-        down = rcopy(buf.at[pl.ds(PAD, PAD)], buf.at[pl.ds(T + PAD, PAD)], previous)
+        up = rcopy(buf.at[:, pl.ds(T, PAD)], buf.at[:, pl.ds(0, PAD)], following)
+        down = rcopy(buf.at[:, pl.ds(PAD, PAD)], buf.at[:, pl.ds(T + PAD, PAD)], previous)
         return up, down
 
     def halo_finish(buf, pair):
@@ -224,14 +263,16 @@
 
         @pl.when(sp == 0)
         def _():
-            buf[0:PAD, :] = jnp.zeros((PAD, C), F32)
+            buf[:, 0:PAD, :] = jnp.zeros((4, PAD, 128), F32)
 
         @pl.when(sp == 15)
         def _():
-            buf[T + PAD:T + 2 * PAD, :] = jnp.zeros((PAD, C), F32)
+            buf[:, T + PAD:T + 2 * PAD, :] = jnp.zeros((4, PAD, 128), F32)
 
     mark("g0")
     halo = halo_start(HID)
+    exchange(y + 1 + 2 * c)
+    exchange(y + 2)
     loads[4].wait()
     mm(G, wo, 0, 0, 0, 256, 0, 2)
     gg_.d0.wait_recv()
@@ -246,14 +287,9 @@
 
     def conv_tile(src, r0, cs, flip):
         acc = jnp.zeros((R, 128), F32)
-        window = src.at[pl.ds(r0, R + 2 * PAD)]
-        for b in range(8):
-            v = window[b:b + R + 24, cs:cs + 128]
-            for a in range(4):
-                o = 8 * a + b
-                if o:
-                    k = TAPS - o if flip else o - 1
-                    acc = acc + TF[k:k + 1, cs:cs + 128] * v[8 * a:8 * a + R]
+        for o in range(1, TAPS + 1):
+            k = TAPS - o if flip else o - 1
+            acc = acc + TF[k:k + 1, cs:cs + 128] * src[cs // 128, pl.ds(r0 + o, R), :]
         return acc
 
     def conv_body(i, _):
@@ -363,16 +399,15 @@
     me_p = (x, z)
     me_q = (z, x)
 
-    def dw(lhs, units, left, h, dp):
-        p = (me_p[h] + dp) % 4
-
-        def body(q, _):
-            zz, xx = (q, p) if h == 0 else (p, q)
-            s = zz * 4 + xx
-            cols = pl.ds(pl.multiple_of((s % 2) * 256, 256), 256)
-            r = dot_nn(left(h), lhs[s // 2, :, cols]).astype(BF16)
-            for n, u in enumerate(units):
-                part[u, h, p, q] = r[n * 256:n * 256 + 256]
+    def dw(lhs, units, left, pair):
+        def body(zz, _):
+            for e in (0, 1):
+                r = dot_nn(left, lhs[zz * 2 + pair, :, e * 256:e * 256 + 256]).astype(BF16)
+                for n, u in enumerate(units):
+                    a = r[n * 512:n * 512 + 256]
+                    b = r[n * 512 + 256:n * 512 + 512]
+                    part[u, 0, 2 * pair + e, zz] = a
+                    part[u, 1, zz, 2 * pair + e] = b
             return 0
 
         lax.fori_loop(0, 4, body, 0)
@@ -456,27 +491,23 @@
                 )
                 w_out[u, :, h * 256 + i:h * 256 + i + 128] = v.T.astype(BF16)
 
-    sc = [[Scatter(u, h) for h in (0, 1)] for u in range(3)]
+    sc = [[Scatter(0, h) for h in (0, 1)]]
 
     def produce(lhs, units, left):
-        for h in (0, 1):
-            dw(lhs, units, left, h, 2)
-            for u in units:
-                sc[u][h].s1()
-        for h in (0, 1):
-            dw(lhs, units, left, h, 1)
-            dw(lhs, units, left, h, 3)
-            for u in units:
-                sc[u][h].s2i()
-        for h in (0, 1):
-            dw(lhs, units, left, h, 0)
+        pair = x // 2
+        dw(lhs, units, left[...], 1 - pair)
+        for u in units:
+            sc[u][0].s1()
+        dw(lhs, units, left[...], pair)
+        for u in units:
+            sc[u][1].s1()
 
     def flip(src, dst, k):
         for cs in COLS:
-            dst[cs // 256, k + cs % 256:k + cs % 256 + 128, :] = src[:, cs:cs + 128].T
+            dst[k + cs:k + cs + 128, :] = src[:, cs:cs + 128].T
 
     flip(ACT, AT, 0)
-    produce(G, [0], lambda h: AT[h])
+    produce(G, [0], AT)
     mark("stats2w")
     stats_finish(1, stats)
 
@@ -487,26 +518,23 @@
         f, s, iv = SA[rows, :], SQ[rows, :], INV[rows, :]
         for cs in COLS:
             col = slice(cs, cs + 128)
-            GC[out_rows, col] = iv * (GA[rows, col] - f - NRM[rows, col] * s)
+            GC[cs // 128, out_rows, :] = iv * (GA[rows, col] - f - NRM[rows, col] * s)
         return 0
 
     lax.fori_loop(0, T // 32, gc_body, 0)
     halo = halo_start(GC)
+    for h in (0, 1):
+        sc[0][h].s2i()
 
     mark("taps")
     for cs in COLS:
         def tap_body(i, accs, cs=cs):
             r0 = pl.multiple_of(i * 32, 32)
-            window = HID.at[pl.ds(r0, 32 + 2 * PAD)]
-            g = GC[pl.ds(pl.multiple_of(r0 + PAD, 16), 32), cs:cs + 128]
+            g = GC[cs // 128, pl.ds(r0 + PAD, 32), :]
             accs = list(accs)
-            for b in range(8):
-                v = window[b:b + 56, cs:cs + 128]
-                for a in range(4):
-                    o = 8 * a + b
-                    if o:
-                        prod = v[8 * a:8 * a + 32] * g
-                        accs[o - 1] = accs[o - 1] + prod.reshape(4, 8, 128).sum(axis=0)
+            for o in range(1, TAPS + 1):
+                prod = HID[cs // 128, pl.ds(r0 + o, 32), :] * g
+                accs[o - 1] = accs[o - 1] + prod.reshape(4, 8, 128).sum(axis=0)
             return tuple(accs)
 
         accs = lax.fori_loop(
@@ -534,6 +562,8 @@
 
     for h in (0, 1):
         sc[0][h].s2d()
+    mark("relay")
+    relays = exchange_relay()
     mark("halo2w")
     halo_finish(GC, halo)
 
@@ -552,14 +582,115 @@
 
     lax.fori_loop(0, T // R, back_body, 0)
 
-    mark("vg_dw")
-    flip(GV, BT, 0)
-    flip(GG, BT, 256)
-    produce(X, [1, 2], lambda h: BT[h])
-
-    mark("ow_p1")
-    for h in (0, 1):
-        sc[0][h].p1()
+    mark("vg_t")
+    for src, k in ((GV, 0), (GG, 256)):
+        for cs in COLS:
+            r = k + cs % 256
+            BT[cs // 256, r:r + 128, :] = src[:, cs:cs + 128].T
+
+    class Spread:
+        def __init__(self, h):
+            self.h, self.p = h, me_p[h]
+
+        def start(self):
+            h, p = self.h, self.p
+            own, got = BT.at[h], BTR.at[h]
+            nxt, prv = at_p[h](p + 1), at_p[h](p + 3)
+            self.h1p = rcopy(own.at[LO], got.at[0, LO], nxt)
+            self.h1m = rcopy(own.at[HIH], got.at[2, HIH], prv)
+            self.h2p = rcopy(own.at[HIH], got.at[0, HIH], nxt)
+            self.h2m = rcopy(own.at[LO], got.at[2, LO], prv)
+
+        def first(self):
+            h, p = self.h, self.p
+            got = BTR.at[h]
+            self.h1p.wait_recv()
+            self.fp = rcopy(got.at[0, LO], got.at[1, LO], at_p[h](p + 1))
+            self.h1m.wait_recv()
+            self.fm = rcopy(got.at[2, HIH], got.at[1, HIH], at_p[h](p + 3))
+
+        def second(self):
+            self.h2p.wait_recv()
+            self.h2m.wait_recv()
+
+        def third(self):
+            self.fp.wait_recv()
+            self.fm.wait_recv()
+
+    def own_in(h, q):
+        zz, xx = (q, x) if h == 0 else (z, q)
+        cols = pl.ds(pl.multiple_of((xx % 2) * 256, 256), 256)
+        return X[zz * 2 + xx // 2, :, cols]
+
+    def got_in(h, k, q):
+        if h == 0:
+            return XA[k, q]
+        return XB[k, q // 2, :, pl.ds(pl.multiple_of((q % 2) * 256, 256), 256)]
+
+    def vg_own(h):
+        def body(q, _):
+            VACC[h, q] = dot_nn(BT[h], own_in(h, q))
+            return 0
+
+        lax.fori_loop(0, 4, body, 0)
+
+    def vg_near(h):
+        def body(q, _):
+            VACC[h, q] += dot_nn(BTR[h, 0], got_in(h, 0, q)) + dot_nn(BTR[h, 2], got_in(h, 2, q))
+            return 0
+
+        lax.fori_loop(0, 4, body, 0)
+
+    class Last:
+        def __init__(self, h):
+            self.h, self.q = h, me_q[h]
+
+        def make(self, dq):
+            h = self.h
+            qq = (self.q + dq) % 4
+            VP[h, qq] = (VACC[h, qq] + dot_nn(BTR[h, 1], got_in(h, 1, qq))).astype(BF16)
+
+        def s1(self):
+            h, q = self.h, self.q
+            src = VP.at[h, (q + 2) % 4]
+            self.i = rcopy(src.at[LO], r3v.at[h, 0], at_q[h](q + 1))
+            self.j = rcopy(src.at[HIH], r3v.at[h, 1], at_q[h](q + 3))
+
+        def s2(self):
+            h, q = self.h, self.q
+
+            def add(qq, row0, k):
+                def body(i, _):
+                    rr = pl.ds(pl.multiple_of(row0 + i * 64, 64), 64)
+                    fr = pl.ds(pl.multiple_of(i * 64, 64), 64)
+                    VP[h, qq, rr] = (VP[h, qq, rr].astype(F32) + r3v[h, k, fr].astype(F32)).astype(BF16)
+                    return 0
+
+                lax.fori_loop(0, 4, body, 0)
+
+            up, down = (q + 1) % 4, (q + 3) % 4
+            self.i.wait_recv()
+            add(up, 0, 0)
+            self.k = rcopy(VP.at[h, up], r4v.at[h, 0], at_q[h](q + 1))
+            self.j.wait_recv()
+            add(down, 256, 1)
+            self.l = rcopy(VP.at[h, down], r4v.at[h, 1], at_q[h](q + 3))
+
+        def finish(self):
+            h, q = self.h, self.q
+            self.k.wait_recv()
+            self.l.wait_recv()
+            for u in (1, 2):
+                for i in (0, 128):
+                    r = (u - 1) * 256 + i
+                    rr = slice(r, r + 128)
+                    v = VP[h, q, rr].astype(F32) + r4v[h, 0, rr].astype(F32) + r4v[h, 1, rr].astype(F32)
+                    w_out[u, :, h * 256 + i:h * 256 + i + 128] = v.T.astype(BF16)
+
+    spread = [Spread(0), Spread(1)]
+    last = [Last(0), Last(1)]
+    for h in (0, 1):
+        spread[h].start()
     TG[1] = small_finish(0, small).astype(BF16)
     small = small_start(1, z, at_z)
 
@@ -585,10 +716,6 @@
 
     partial(1 - c)
     swap = rcopy(G.at[pl.ds((1 - c) * 4, 4)], PR, partner)
-    mark("vg_s2d")
-    for u in (1, 2):
-        for h in (0, 1):
-            sc[u][h].s2d()
     mark("partial2")
     partial(c)
     mark("yadd")
@@ -616,9 +743,23 @@
     yd = rcopy(G.at[base + ym_, LO], y2.at[1, LO], at_y(y + 3))
     y_add(base + y, 0, T, [(PR, (y,), 0)])
 
-    mark("ow_p2")
-    for h in (0, 1):
-        sc[0][h].p2()
+    mark("vg_first")
+    for h in (0, 1):
+        spread[h].first()
+    mark("vg_own")
+    for h in (0, 1):
+        vg_own(h)
+    mark("ow_p1")
+    for h in (0, 1):
+        sc[0][h].p1()
+    for cp in relays:
+        cp.wait_recv()
+    mark("vg_second")
+    for h in (0, 1):
+        spread[h].second()
+    mark("vg_near")
+    for h in (0, 1):
+        vg_near(h)
     mark("y_s2")
     ya.wait_recv()
     y_add(base + yp_, 0, 256, [(y1, (0,), 0)])
@@ -626,24 +767,29 @@
     yb.wait_recv()
     y_add(base + ym_, 256, 256, [(y1, (1,), 0)])
     yf = rcopy(G.at[base + ym_, HIH], y2.at[1, HIH], at_y(y + 3))
-
-    mark("v_p1")
-    for h in (0, 1):
-        sc[1][h].p1()
+    mark("vg_third")
+    for h in (0, 1):
+        spread[h].third()
+    mark("vg_far")
+    for h in (0, 1):
+        last[h].make(2)
+        last[h].s1()
+    for dq in (1, 3):
+        for h in (0, 1):
+            last[h].make(dq)
+    mark("ow_p2")
+    for h in (0, 1):
+        sc[0][h].p2()
+    mark("vg_s2")
+    for h in (0, 1):
+        last[h].s2()
+    mark("vg_mine")
+    for h in (0, 1):
+        last[h].make(0)
     mark("ow_fin")
     for h in (0, 1):
         sc[0][h].finish()
-    total = small_finish(1, small)
-    taps_out[...] = total
-    mark("g_p1")
-    for h in (0, 1):
-        sc[2][h].p1()
-    mark("v_p2")
-    for h in (0, 1):
-        sc[1][h].p2()
-    mark("g_p2")
-    for h in (0, 1):
-        sc[2][h].p2()
+    small_out[...] = small_finish(1, small)
     mark("y_fin")
     for cp in (yc, yd, ye, yf):
         cp.wait_recv()
@@ -658,13 +804,13 @@
     lax.fori_loop(0, T // 32, gi_body, 0)
     mark("fin")
     for h in (0, 1):
-        sc[1][h].finish()
-    for h in (0, 1):
-        sc[2][h].finish()
+        last[h].finish()
     mark("sends")
     for cp in sent:
         if id(cp) not in done:
             cp.wait_send()
+    for d in (1, 2, 3):
+        ex_b(d, (z + d) % 4).wait_send()
     mark(None)
     assert counter[0] <= N_COPIES, counter[0]
 
@@ -712,19 +858,23 @@
             vm((NB, T, C), BF16), vm((NB, T, C), BF16),
             vm(shape3, BF16), vm(shape3, BF16), vm(shape3, BF16),
             vm((T, C), F32), vm((T, C), F32), vm((T, C), F32), vm((T, C), F32),
-            vm((T + 2 * PAD, C), F32), vm((T + 2 * PAD, C), F32),
+            vm((4, T + 2 * PAD, 128), F32), vm((4, T + 2 * PAD, 128), F32),
             vm((T, C), BF16), vm((T, C), BF16), vm((T, C), BF16),
-            vm((2, 256, T), BF16), vm((2, 512, T), BF16),
+            vm((512, T), BF16), vm((2, 512, T), BF16),
             vm((T, 128), F32), vm((T, 128), F32), vm((T, 128), F32), vm((T, 128), F32),
             vm((32, C), F32),
             vm((2, 8, T), F32), vm((2, NB, 8, T), F32),
             vm((32, C), F32), vm((8, C), F32),
             vm((2, 32, C), BF16), vm((2, 4, 32, C), BF16),
-            vm((3, 2, 4, 4, 256, 256), BF16),
-            vm((3, 2, 2, 2, 256, 256), BF16),
-            vm((3, 2, 2, 4, 256, 256), BF16),
-            vm((3, 2, 2, 128, 256), BF16),
-            vm((3, 2, 2, 256, 256), BF16),
+            vm((1, 2, 4, 4, 256, 256), BF16),
+            vm((1, 2, 2, 2, 256, 256), BF16),
+            vm((1, 2, 2, 4, 256, 256), BF16),
+            vm((1, 2, 2, 128, 256), BF16),
+            vm((1, 2, 2, 256, 256), BF16),
+            vm((3, 4, T, 256), BF16), vm((3, 2, T, C), BF16),
+            vm((2, 3, 512, T), BF16),
+            vm((2, 4, 512, 256), F32), vm((2, 4, 512, 256), BF16),
+            vm((2, 2, 256, 256), BF16), vm((2, 2, 512, 256), BF16),
             vm((4, T, C), BF16),
             vm((2, 256, C), BF16), vm((2, T, C), BF16),
             pltpu.SemaphoreType.DMA((N_COPIES,)),

time: 134 us -> 114 us (0.85)
  Pallas kernels: 133 us -> 113 us
    pallas_call x1, Pallas kernels: 130 us -> 110 us  [local(): pl.pallas_call(kernel, out_shape=(jax.ShapeDtypeStruct((T, C), BF16), jax...]
where the time goes in v3:
time: 114 us
  Pallas kernels  113 us (99%)
    pallas_call x1, Pallas kernels, local(): pl.pallas_call(kernel, out_shape=(jax.ShapeDtypeStruct((T, C), BF16), jax...  110 us
    pallas_call x1, Pallas kernels, local(): pl.pallas_call(unpack, out_shape=(jax.ShapeDtypeStruct((T, C), BF16), jax...  3.01 us

profile of v3, /device:TPU:1, one launch (start us, length us, event | category | flops | bytes accessed | tf_op | source)
XLA Modules:
  0.0 113.7 jit_solution(8171453644555779373)
XLA Ops:
  0.6 109.9 %shard_map.118 = (bf16[512,512]{1,0:T(8,128)(2,1)}, bf16[3,256,512]{2,1,0:T(8,128)(2,1)}, f32[32,512]{1,0:T(8,128)}) custom-call(bf16[512,512]{1,0:T(8,128)(2,1)} %x_hbm.1, bf16[512,512]{1,0:T(8,128)(2,1)} %g_hbm.1, bf16[8,512,512]{2,1,0:T(8,128)(2,1)} %bitcast.5, bf16[8,512,512]{2,1,0:T(8,128)(2,1)} %bitcast.6, bf16[8,512,512]{2,1,0:T(8,128)(2,1)} %bitcast.7, ...), custom_call_target="tpu_custom_call" | custom-call | tf_op jit(solution)/shard_map/pallas_call | solution.py:848
  110.5 3.0 %shard_map.119 = (bf16[512,512]{1,0:T(8,128)(2,1)}, f32[256,512]{1,0:T(8,128)}, f32[256,512]{1,0:T(8,128)}, f32[256,512]{1,0:T(8,128)}, f32[31,512]{1,0:T(8,128)}, /*index=5*/f32[1,512]{1,0:T(1,128)}) custom-call(bf16[512,512]{1,0:T(8,128)(2,1)} %get-tuple-element.15.gi_in, bf16[3,256,512]{2,1,0:T(8,128)(2,1)} %get-tuple-element.16.w_in, ...), custom_call_target="tpu_custom_call" | custom-call | tf_op jit(solution)/shard_map/pallas_call | solution.py:891

commit v4 on v3

--- a/solution.py
+++ b/solution.py
@@ -39,7 +39,7 @@
     x_hbm, g_hbm, wv_hbm, wg_hbm, wo_hbm, taps_ref, gain_ref,
     gi_out, w_out, small_out,
     X, G, WV, WG, WO, PV, PG, GA, NRM, HID, GC, ACT, GV, GG, AT, BT,
-    SA, SQ, MEAN, INV, TF, ST, STR, TP, GP, TG, TGR,
+    SA, SQ, MEAN, INV, TF, ST, STR, TP, GP, TG, TG1, TGR,
     part, r1, r2, r3, r4, XA, XB, BTR, VACC, VP, r3v, r4v, PR, y1, y2, ss, rs, ls,
 ):
     sp = lax.axis_index("sp")
@@ -493,21 +493,18 @@
 
     sc = [[Scatter(0, h) for h in (0, 1)]]
 
-    def produce(lhs, units, left):
-        pair = x // 2
-        dw(lhs, units, left[...], 1 - pair)
-        for u in units:
-            sc[u][0].s1()
-        dw(lhs, units, left[...], pair)
-        for u in units:
-            sc[u][1].s1()
-
-    def flip(src, dst, k):
-        for cs in COLS:
-            dst[k + cs:k + cs + 128, :] = src[:, cs:cs + 128].T
-
-    flip(ACT, AT, 0)
-    produce(G, [0], AT)
+    def flipped(src, n):
+        eye = (
+            lax.broadcasted_iota(jnp.int32, (256, 256), 0) == lax.broadcasted_iota(jnp.int32, (256, 256), 1)
+        ).astype(F32).astype(BF16)
+        return dot_nt(eye, src[:, n:n + 256]).astype(BF16)
+
+    for n in (0, 256):
+        AT[n:n + 256, :] = flipped(ACT, n)
+    dw(G, [0], AT[...], 1 - x // 2)
+    sc[0][0].s1()
+    mark("ow_dw2")
+    dw(G, [0], AT[...], x // 2)
     mark("stats2w")
     stats_finish(1, stats)
 
@@ -523,6 +520,7 @@
 
     lax.fori_loop(0, T // 32, gc_body, 0)
     halo = halo_start(GC)
+    sc[0][1].s1()
     for h in (0, 1):
         sc[0][h].s2i()
 
@@ -544,24 +542,21 @@
             TP[k:k + 1, cs:cs + 128] = jnp.sum(a, axis=0, keepdims=True)
     TP[TAPS:TAPS + 1, :] = jnp.sum(GP[...], axis=0, keepdims=True)
 
-    def small_start(e, me, at):
-        TGR[e, me] = TG[e]
-        return [rcopy(TG.at[e], TGR.at[e, me], at(me + d)) for d in range(1, 4)]
-
-    def small_finish(e, copies):
+    def small_send(e, src, me, at):
+        TGR[e, me] = src(me)[...]
+        return [rcopy(src((me + d) % 4), TGR.at[e, me], at(me + d)) for d in (1, 3, 2)]
+
+    def small_sum(e, copies):
         for cp in copies:
             cp.wait_recv()
         v = TGR[e, 0].astype(F32)
         for i in range(1, 4):
             v = v + TGR[e, i].astype(F32)
-        return v
-
-    mark("ow_s2d")
-    TG[0] = TP[...].astype(BF16)
-    small = small_start(0, x, at_x)
-
-    for h in (0, 1):
-        sc[0][h].s2d()
+        return v.astype(BF16)
+
+    for t in range(4):
+        TG[t] = TP[:, t * 128:t * 128 + 128].astype(BF16)
+    small = small_send(0, lambda t: TG.at[t], x, at_x)
     mark("relay")
     relays = exchange_relay()
     mark("halo2w")
@@ -583,31 +578,30 @@
     lax.fori_loop(0, T // R, back_body, 0)
 
     mark("vg_t")
-    for src, k in ((GV, 0), (GG, 256)):
-        for cs in COLS:
-            r = k + cs % 256
-            BT[cs // 256, r:r + 128, :] = src[:, cs:cs + 128].T
+    for n in (0, 256):
+        BT[n // 256, 0:256, :] = flipped(GV, n)
 
     class Spread:
-        def __init__(self, h):
+        def __init__(self, h, u):
             self.h, self.p = h, me_p[h]
+            self.lo, self.hi = pl.ds(u * 256, 128), pl.ds(u * 256 + 128, 128)
 
         def start(self):
-            h, p = self.h, self.p
+            h, p, lo, hi = self.h, self.p, self.lo, self.hi
             own, got = BT.at[h], BTR.at[h]
             nxt, prv = at_p[h](p + 1), at_p[h](p + 3)
-            self.h1p = rcopy(own.at[LO], got.at[0, LO], nxt)
-            self.h1m = rcopy(own.at[HIH], got.at[2, HIH], prv)
-            self.h2p = rcopy(own.at[HIH], got.at[0, HIH], nxt)
-            self.h2m = rcopy(own.at[LO], got.at[2, LO], prv)
+            self.h1p = rcopy(own.at[lo], got.at[0, lo], nxt)
+            self.h1m = rcopy(own.at[hi], got.at[2, hi], prv)
+            self.h2p = rcopy(own.at[hi], got.at[0, hi], nxt)
+            self.h2m = rcopy(own.at[lo], got.at[2, lo], prv)
 
         def first(self):
-            h, p = self.h, self.p
+            h, p, lo, hi = self.h, self.p, self.lo, self.hi
             got = BTR.at[h]
             self.h1p.wait_recv()
-            self.fp = rcopy(got.at[0, LO], got.at[1, LO], at_p[h](p + 1))
+            self.fp = rcopy(got.at[0, lo], got.at[1, lo], at_p[h](p + 1))
             self.h1m.wait_recv()
-            self.fm = rcopy(got.at[2, HIH], got.at[1, HIH], at_p[h](p + 3))
+            self.fm = rcopy(got.at[2, hi], got.at[1, hi], at_p[h](p + 3))
 
         def second(self):
             self.h2p.wait_recv()
@@ -634,65 +628,66 @@
 
         lax.fori_loop(0, 4, body, 0)
 
-    def vg_near(h):
+    def vg_near(h, u):
+        rows = pl.ds(u * 256, 256)
+
         def body(q, _):
-            VACC[h, q] += dot_nn(BTR[h, 0], got_in(h, 0, q)) + dot_nn(BTR[h, 2], got_in(h, 2, q))
+            VACC[h, q, rows] += dot_nn(BTR[h, 0, rows], got_in(h, 0, q)) + dot_nn(BTR[h, 2, rows], got_in(h, 2, q))
             return 0
 
         lax.fori_loop(0, 4, body, 0)
 
     class Last:
-        def __init__(self, h):
-            self.h, self.q = h, me_q[h]
+        def __init__(self, h, u):
+            self.h, self.u, self.q = h, u, me_q[h]
+            self.rows = pl.ds(u * 256, 256)
 
         def make(self, dq):
-            h = self.h
+            h, rows = self.h, self.rows
             qq = (self.q + dq) % 4
-            VP[h, qq] = (VACC[h, qq] + dot_nn(BTR[h, 1], got_in(h, 1, qq))).astype(BF16)
+            VP[h, qq, rows] = (VACC[h, qq, rows] + dot_nn(BTR[h, 1, rows], got_in(h, 1, qq))).astype(BF16)
 
         def s1(self):
-            h, q = self.h, self.q
+            h, u, q = self.h, self.u, self.q
             src = VP.at[h, (q + 2) % 4]
-            self.i = rcopy(src.at[LO], r3v.at[h, 0], at_q[h](q + 1))
-            self.j = rcopy(src.at[HIH], r3v.at[h, 1], at_q[h](q + 3))
+            self.i = rcopy(src.at[pl.ds(u * 256, 128)], r3v.at[h, u, 0], at_q[h](q + 1))
+            self.j = rcopy(src.at[pl.ds(u * 256 + 128, 128)], r3v.at[h, u, 1], at_q[h](q + 3))
 
         def s2(self):
-            h, q = self.h, self.q
+            h, u, q, rows = self.h, self.u, self.q, self.rows
 
             def add(qq, row0, k):
                 def body(i, _):
                     rr = pl.ds(pl.multiple_of(row0 + i * 64, 64), 64)
                     fr = pl.ds(pl.multiple_of(i * 64, 64), 64)
-                    VP[h, qq, rr] = (VP[h, qq, rr].astype(F32) + r3v[h, k, fr].astype(F32)).astype(BF16)
+                    VP[h, qq, rr] = (VP[h, qq, rr].astype(F32) + r3v[h, u, k, fr].astype(F32)).astype(BF16)
                     return 0
 
-                lax.fori_loop(0, 4, body, 0)
+                lax.fori_loop(0, 2, body, 0)
 
             up, down = (q + 1) % 4, (q + 3) % 4
             self.i.wait_recv()
-            add(up, 0, 0)
-            self.k = rcopy(VP.at[h, up], r4v.at[h, 0], at_q[h](q + 1))
+            add(up, u * 256, 0)
+            self.k = rcopy(VP.at[h, up, rows], r4v.at[h, 0, rows], at_q[h](q + 1))
             self.j.wait_recv()
-            add(down, 256, 1)
-            self.l = rcopy(VP.at[h, down], r4v.at[h, 1], at_q[h](q + 3))
+            add(down, u * 256 + 128, 1)
+            self.l = rcopy(VP.at[h, down, rows], r4v.at[h, 1, rows], at_q[h](q + 3))
 
         def finish(self):
-            h, q = self.h, self.q
+            h, u, q = self.h, self.u, self.q
             self.k.wait_recv()
             self.l.wait_recv()
-            for u in (1, 2):
-                for i in (0, 128):
-                    r = (u - 1) * 256 + i
-                    rr = slice(r, r + 128)
-                    v = VP[h, q, rr].astype(F32) + r4v[h, 0, rr].astype(F32) + r4v[h, 1, rr].astype(F32)
-                    w_out[u, :, h * 256 + i:h * 256 + i + 128] = v.T.astype(BF16)
-
-    spread = [Spread(0), Spread(1)]
-    last = [Last(0), Last(1)]
-    for h in (0, 1):
-        spread[h].start()
-    TG[1] = small_finish(0, small).astype(BF16)
-    small = small_start(1, z, at_z)
+            for i in (0, 128):
+                rr = slice(u * 256 + i, u * 256 + i + 128)
+                v = VP[h, q, rr].astype(F32) + r4v[h, 0, rr].astype(F32) + r4v[h, 1, rr].astype(F32)
+                w_out[u + 1, :, h * 256 + i:h * 256 + i + 128] = v.T.astype(BF16)
+
+    spread = [[Spread(0, u), Spread(1, u)] for u in (0, 1)]
+    last = [[Last(0, u), Last(1, u)] for u in (0, 1)]
+    for h in (0, 1):
+        spread[0][h].start()
+    for n in (0, 256):
+        BT[n // 256, 256:512, :] = flipped(GG, n)
 
     mark("partial1")
     for cp in (gg_.h1p, gg_.h1m, gg_.d0, gg_.h2p, gg_.h2m, gg_.fp, gg_.fm, gg_.d1p, gg_.d1m,
@@ -716,6 +711,11 @@
 
     partial(1 - c)
     swap = rcopy(G.at[pl.ds((1 - c) * 4, 4)], PR, partner)
+    mark("v_first")
+    for h in (0, 1):
+        spread[0][h].first()
+    for h in (0, 1):
+        spread[1][h].start()
     mark("partial2")
     partial(c)
     mark("yadd")
@@ -743,23 +743,32 @@
     yd = rcopy(G.at[base + ym_, LO], y2.at[1, LO], at_y(y + 3))
     y_add(base + y, 0, T, [(PR, (y,), 0)])
 
-    mark("vg_first")
-    for h in (0, 1):
-        spread[h].first()
     mark("vg_own")
     for h in (0, 1):
         vg_own(h)
-    mark("ow_p1")
-    for h in (0, 1):
-        sc[0][h].p1()
+    mark("g_first")
+    for h in (0, 1):
+        spread[1][h].first()
+    mark("ow_s2d")
+    for h in (0, 1):
+        sc[0][h].s2d()
     for cp in relays:
         cp.wait_recv()
-    mark("vg_second")
-    for h in (0, 1):
-        spread[h].second()
-    mark("vg_near")
-    for h in (0, 1):
-        vg_near(h)
+    mark("v_near")
+    for h in (0, 1):
+        spread[0][h].second()
+    for h in (0, 1):
+        vg_near(h, 0)
+    mark("v_third")
+    for h in (0, 1):
+        spread[0][h].third()
+    mark("v_far")
+    for h in (0, 1):
+        last[0][h].make(2)
+        last[0][h].s1()
+    for dq in (1, 3, 0):
+        for h in (0, 1):
+            last[0][h].make(dq)
     mark("y_s2")
     ya.wait_recv()
     y_add(base + yp_, 0, 256, [(y1, (0,), 0)])
@@ -767,29 +776,43 @@
     yb.wait_recv()
     y_add(base + ym_, 256, 256, [(y1, (1,), 0)])
     yf = rcopy(G.at[base + ym_, HIH], y2.at[1, HIH], at_y(y + 3))
-    mark("vg_third")
-    for h in (0, 1):
-        spread[h].third()
-    mark("vg_far")
-    for h in (0, 1):
-        last[h].make(2)
-        last[h].s1()
-    for dq in (1, 3):
+    mark("small")
+    TG1[0] = small_sum(0, small)
+    small = small_send(1, lambda t: TG1.at[0], z, at_z)
+    mark("g_second")
+    for h in (0, 1):
+        spread[1][h].second()
+    mark("g_near")
+    for h in (0, 1):
+        vg_near(h, 1)
+    mark("g_third")
+    for h in (0, 1):
+        spread[1][h].third()
+    mark("g_far")
+    for h in (0, 1):
+        last[1][h].make(2)
+        last[1][h].s1()
+    for dq in (1, 3, 0):
         for h in (0, 1):
-            last[h].make(dq)
+            last[1][h].make(dq)
+    mark("ow_p1")
+    for h in (0, 1):
+        sc[0][h].p1()
+    TG1[1] = small_sum(1, small)
+    small = small_send(2, lambda t: TG1.at[1], x, at_x)
+    mark("v_s2")
+    for h in (0, 1):
+        last[0][h].s2()
+    mark("g_s2")
+    for h in (0, 1):
+        last[1][h].s2()
     mark("ow_p2")
     for h in (0, 1):
         sc[0][h].p2()
-    mark("vg_s2")
-    for h in (0, 1):
-        last[h].s2()
-    mark("vg_mine")
-    for h in (0, 1):
-        last[h].make(0)
-    mark("ow_fin")
-    for h in (0, 1):
-        sc[0][h].finish()
-    small_out[...] = small_finish(1, small)
+    for cp in small:
+        cp.wait_recv()
+    for t in range(4):
+        small_out[:, t * 128:t * 128 + 128] = TGR[2, t].astype(F32)
     mark("y_fin")
     for cp in (yc, yd, ye, yf):
         cp.wait_recv()
@@ -804,7 +827,13 @@
     lax.fori_loop(0, T // 32, gi_body, 0)
     mark("fin")
     for h in (0, 1):
-        last[h].finish()
+        last[0][h].finish()
+    mark("g_fin")
+    for h in (0, 1):
+        last[1][h].finish()
+    mark("ow_fin")
+    for h in (0, 1):
+        sc[0][h].finish()
     mark("sends")
     for cp in sent:
         if id(cp) not in done:
@@ -815,27 +844,15 @@
     assert counter[0] <= N_COPIES, counter[0]
 
 
-def unpack(gi_in, w_in, small_in, gi, gvw, ggw, gow, gt, gg, b_gi, b_in, b_out, b_small, si, so):
-    reads = [
-        pltpu.make_async_copy(w_in.at[u], b_in.at[u], si.at[u]) for u in range(3)
-    ] + [
-        pltpu.make_async_copy(gi_in, b_gi, si.at[3]),
-        pltpu.make_async_copy(small_in, b_small, si.at[4]),
-    ]
-    for cp in reads:
-        cp.start()
-    writes = []
+def unpack(gi_in, w_in, small_in, gi, gvw, ggw, gow, gt, gg, b_out, so):
+    writes = [pltpu.make_async_copy(gi_in, gi, so.at[3])]
+    writes[0].start()
     for u, dst in enumerate((gow, gvw, ggw)):
-        reads[u].wait()
-        b_out[u] = b_in[u].astype(F32)
+        b_out[u] = w_in[u].astype(F32)
         writes.append(pltpu.make_async_copy(b_out.at[u], dst, so.at[u]))
         writes[-1].start()
-    reads[3].wait()
-    writes.append(pltpu.make_async_copy(b_gi, gi, so.at[3]))
-    writes[-1].start()
-    reads[4].wait()
-    gt[...] = b_small[0:TAPS]
-    gg[...] = b_small[TAPS:TAPS + 1]
+    gt[...] = small_in[0:TAPS]
+    gg[...] = small_in[TAPS:TAPS + 1]
     for cp in writes:
         cp.wait()
 
@@ -848,9 +865,9 @@
     gi, w3, small = pl.pallas_call(
         kernel,
         out_shape=(
-            jax.ShapeDtypeStruct((T, C), BF16),
-            jax.ShapeDtypeStruct((3, 256, C), BF16),
-            jax.ShapeDtypeStruct((32, C), F32),
+            vm((T, C), BF16),
+            vm((3, 256, C), BF16),
+            vm((32, C), F32),
         ),
         in_specs=[anyspace] * 5 + [in_vmem] * 2,
         out_specs=(in_vmem,) * 3,
@@ -865,7 +882,7 @@
             vm((32, C), F32),
             vm((2, 8, T), F32), vm((2, NB, 8, T), F32),
             vm((32, C), F32), vm((8, C), F32),
-            vm((2, 32, C), BF16), vm((2, 4, 32, C), BF16),
+            vm((4, 32, 128), BF16), vm((2, 32, 128), BF16), vm((3, 4, 32, 128), BF16),
             vm((1, 2, 4, 4, 256, 256), BF16),
             vm((1, 2, 2, 2, 256, 256), BF16),
             vm((1, 2, 2, 4, 256, 256), BF16),
@@ -874,7 +891,7 @@
             vm((3, 4, T, 256), BF16), vm((3, 2, T, C), BF16),
             vm((2, 3, 512, T), BF16),
             vm((2, 4, 512, 256), F32), vm((2, 4, 512, 256), BF16),
-            vm((2, 2, 256, 256), BF16), vm((2, 2, 512, 256), BF16),
+            vm((2, 2, 2, 128, 256), BF16), vm((2, 2, 512, 256), BF16),
             vm((4, T, C), BF16),
             vm((2, 256, C), BF16), vm((2, T, C), BF16),
             pltpu.SemaphoreType.DMA((N_COPIES,)),
@@ -882,7 +899,7 @@
             pltpu.SemaphoreType.DMA((5,)),
         ],
         compiler_params=pltpu.CompilerParams(
-            collective_id=0, has_side_effects=True, vmem_limit_bytes=67043328
+            collective_id=0, has_side_effects=True, vmem_limit_bytes=64 * 1024 * 1024 - 3 * 1024 * 1024
         ),
     )(
         inputs, grad_out, w_value.reshape(shape3), w_gate.reshape(shape3), w_out.reshape(shape3),
@@ -898,12 +915,10 @@
             jax.ShapeDtypeStruct((TAPS, C), F32),
             jax.ShapeDtypeStruct((1, C), F32),
         ),
-        in_specs=[anyspace] * 3,
+        in_specs=[in_vmem] * 3,
         out_specs=(anyspace,) * 4 + (in_vmem,) * 2,
-        scratch_shapes=[
-            vm((T, C), BF16), vm((3, 256, C), BF16), vm((3, 256, C), F32), vm((32, C), F32),
-            pltpu.SemaphoreType.DMA((5,)), pltpu.SemaphoreType.DMA((4,)),
-        ],
+        scratch_shapes=[vm((3, 256, C), F32), pltpu.SemaphoreType.DMA((4,))],
+        compiler_params=pltpu.CompilerParams(vmem_limit_bytes=8 * 1024 * 1024),
     )(gi, w3, small)
     return gi, gvw, ggw, gow, gt, gg.reshape(C)
 

time: 114 us -> 111 us (0.974)
  Pallas kernels: 113 us -> 110 us
    pallas_call x1, Pallas kernels: 110 us -> 108 us  [local(): pl.pallas_call(kernel, out_shape=(vm((T, C), BF16), vm((3, 256, C), BF16)...]
where the time goes in v4:
time: 111 us; the launch traced here: 110 us
  Pallas kernels  110 us (99%)
    pallas_call x1, Pallas kernels, local(): pl.pallas_call(kernel, out_shape=(vm((T, C), BF16), vm((3, 256, C), BF16)...  108 us

profile of v4, /device:TPU:1, one launch (start us, length us, event | category | flops | bytes accessed | tf_op | source)
XLA Modules:
  0.0 110.4 jit_solution(1169480687202202190)
XLA Ops:
  0.6 107.6 %shard_map.118 = (bf16[512,512]{1,0:T(8,128)(2,1)S(1)}, bf16[3,256,512]{2,1,0:T(8,128)(2,1)S(1)}, f32[32,512]{1,0:T(8,128)S(1)}) custom-call(bf16[512,512]{1,0:T(8,128)(2,1)} %x_hbm.1, bf16[512,512]{1,0:T(8,128)(2,1)} %g_hbm.1, bf16[8,512,512]{2,1,0:T(8,128)(2,1)} %bitcast.5, bf16[8,512,512]{2,1,0:T(8,128)(2,1)} %bitcast.6, bf16[8,512,512]{2,1,0:T(8,128)(2,1)} %bitcast.7, ...), custom_call_target="tpu_custom_call" | custom-call | tf_op jit(solution)/shard_map/pallas_call | solution.py:865
  108.3 2.0 %shard_map.119 = (bf16[512,512]{1,0:T(8,128)(2,1)}, f32[256,512]{1,0:T(8,128)}, f32[256,512]{1,0:T(8,128)}, f32[256,512]{1,0:T(8,128)}, f32[31,512]{1,0:T(8,128)}, /*index=5*/f32[1,512]{1,0:T(1,128)}) custom-call(bf16[512,512]{1,0:T(8,128)(2,1)S(1)} %get-tuple-element.15.gi_in, bf16[3,256,512]{2,1,0:T(8,128)(2,1)S(1)} %get-tuple-element.16.w_in, ...), custom_call_target="tpu_custom_call" | custom-call | tf_op jit(solution)/shard_map/pallas_call | solution.py:908

commit v5 on v4

--- a/solution.py
+++ b/solution.py
@@ -16,7 +16,8 @@
 TAPS = 31
 PAD = 16
 COLS = (0, 128, 256, 384)
-N_COPIES = 160
+N_COPIES = 141
+N_SENDS = 76
 
 
 def sig(v):
@@ -36,11 +37,11 @@
 
 
 def kernel(
-    x_hbm, g_hbm, wv_hbm, wg_hbm, wo_hbm, taps_ref, gain_ref,
+    x_hbm, g_hbm, wv_hbm, wg_hbm, wo_hbm, taps_hbm, gain_hbm,
     gi_out, w_out, small_out,
     X, G, WV, WG, WO, PV, PG, GA, NRM, HID, GC, ACT, GV, GG, AT, BT,
     SA, SQ, MEAN, INV, TF, ST, STR, TP, GP, TG, TG1, TGR,
-    part, r1, r2, r3, r4, XA, XB, BTR, VACC, VP, r3v, r4v, PR, y1, y2, ss, rs, ls,
+    part, r1, r2, r3, r4, XA, XB, BTR, VACC, VP, r3v, r4v, PR, y1, y2, taps_ref, gain_ref, ss, rs, ls,
 ):
     sp = lax.axis_index("sp")
     tp = lax.axis_index("tp")
@@ -71,24 +72,32 @@
             scope[0].__enter__()
 
     counter = [0]
+    free = list(range(N_SENDS))
     sent = []
-    done = []
 
     def rcopy(src, dst, dev):
         i = counter[0]
         counter[0] += 1
+        k = free.pop(0)
         cp = pltpu.make_async_remote_copy(
-            src_ref=src, dst_ref=dst, send_sem=ss.at[i], recv_sem=rs.at[i],
+            src_ref=src, dst_ref=dst, send_sem=ss.at[k], recv_sem=rs.at[i],
             device_id=dev, device_id_type=MESH,
         )
         cp.start()
-        sent.append(cp)
+        sent.append((cp, k))
         return cp
+
+    def drain(count):
+        for cp, k in sent[:count]:
+            cp.wait_send()
+            free.append(k)
+        del sent[:count]
 
     mark("entry")
     loads = []
     for i, (src, dst) in enumerate(
-        ((x_hbm, X.at[tp]), (wv_hbm, WV), (wg_hbm, WG), (g_hbm, G.at[tp]), (wo_hbm, WO))
+        ((x_hbm, X.at[tp]), (wv_hbm, WV), (wg_hbm, WG), (g_hbm, G.at[tp]), (wo_hbm, WO),
+         (taps_hbm, taps_ref), (gain_hbm, gain_ref))
     ):
         cp = pltpu.make_async_copy(src, dst, ls.at[i])
         cp.start()
@@ -103,8 +112,6 @@
     PV[...] = jnp.zeros((T, C), F32)
     PG[...] = jnp.zeros((T, C), F32)
     GA[...] = jnp.zeros((T, C), F32)
-    TF[...] = jnp.zeros((32, C), F32)
-    TF[0:TAPS, :] = taps_ref[...].astype(F32)
     pl.semaphore_wait(barrier, len(peers))
 
     jm = ((y + 3) % 4) * 2 + c
@@ -167,11 +174,14 @@
     ex_a = []
     b0 = counter[0]
     counter[0] += 3
+    bs = free[:3]
+    del free[:3]
+    bs0 = bs[0]
 
     def ex_b(d, yy):
         return pltpu.make_async_remote_copy(
             src_ref=X.at[pl.ds(2 * yy, 2), toks], dst_ref=XB.at[d - 1, :, toks],
-            send_sem=ss.at[b0 + d - 1], recv_sem=rs.at[b0 + d - 1],
+            send_sem=ss.at[bs0 + d - 1], recv_sem=rs.at[b0 + d - 1],
             device_id=at_z(z + d), device_id_type=MESH,
         )
 
@@ -238,6 +248,10 @@
     mm(X, vg, 2, 2, 0, 256, 2, 4)
 
     mark("hidden")
+    loads[5].wait()
+    loads[6].wait()
+    TF[...] = jnp.zeros((32, C), F32)
+    TF[0:TAPS, :] = taps_ref[...].astype(F32)
     def hidden_body(i, _):
         rows = pl.ds(pl.multiple_of(i * 32, 32), 32)
         out_rows = pl.ds(pl.multiple_of(i * 32 + PAD, 16), 32)
@@ -316,6 +330,11 @@
         ) + lax.dot_general(
             jnp.where(row == 1, 1.0, 0.0).astype(F32), SQ[...], dims, precision=HI, preferred_element_type=F32
         )
+        packed = jnp.zeros((8, 128), F32)
+        for r in range(4):
+            packed = jnp.where(row == r, tile[0:1, 128 * r:128 * r + 128], packed)
+            packed = jnp.where(row == r + 4, tile[1:2, 128 * r:128 * r + 128], packed)
+        tile = packed
         ST[e] = tile
         STR[e, tp] = tile
         return [rcopy(ST.at[e], STR.at[e, tp], at_tp((tp + d) % 8)) for d in range(1, 8)]
@@ -325,10 +344,10 @@
             cp.wait_recv()
         row = lax.broadcasted_iota(jnp.int32, (64, 256), 0) & 7
         lane = lax.broadcasted_iota(jnp.int32, (64, 256), 1)
-        want = jnp.where(lane < 128, 0, 1)
-        pick = jnp.where(row == want, 1.0, 0.0).astype(F32)
+        want = jnp.where(lane < 128, 0, 4)
+        block = STR[e].reshape(64, 128)
         for t in range(0, T, 128):
-            block = STR[e, :, :, t:t + 128].reshape(64, 128)
+            pick = jnp.where(row == want + t // 128, 1.0, 0.0).astype(F32)
             both = lax.dot_general(
                 block, pick, (((0,), (0,)), ((), ())), precision=HI, preferred_element_type=F32
             ) * (1.0 / (NB * C))
@@ -391,6 +410,7 @@
         return 0
 
     lax.fori_loop(0, T // 32, scaled_body, 0)
+    early = len(sent)
     mark("stats2")
     stats = stats_start(1)
 
@@ -399,8 +419,9 @@
     me_p = (x, z)
     me_q = (z, x)
 
-    def dw(lhs, units, left, pair):
-        def body(zz, _):
+    def dw(lhs, units, left, pair, lo=0, hi=4):
+        def body(k, _):
+            zz = (z + 2 + k) % 4
             for e in (0, 1):
                 r = dot_nn(left, lhs[zz * 2 + pair, :, e * 256:e * 256 + 256]).astype(BF16)
                 for n, u in enumerate(units):
@@ -410,7 +431,7 @@
                     part[u, 1, zz, 2 * pair + e] = b
             return 0
 
-        lax.fori_loop(0, 4, body, 0)
+        lax.fori_loop(lo, hi, body, 0)
 
     class Scatter:
         def __init__(self, u, h):
@@ -504,7 +525,9 @@
     dw(G, [0], AT[...], 1 - x // 2)
     sc[0][0].s1()
     mark("ow_dw2")
-    dw(G, [0], AT[...], x // 2)
+    dw(G, [0], AT[...], x // 2, 0, 1)
+    sc[0][1].s1()
+    dw(G, [0], AT[...], x // 2, 1, 4)
     mark("stats2w")
     stats_finish(1, stats)
 
@@ -520,7 +543,6 @@
 
     lax.fori_loop(0, T // 32, gc_body, 0)
     halo = halo_start(GC)
-    sc[0][1].s1()
     for h in (0, 1):
         sc[0][h].s2i()
 
@@ -559,6 +581,7 @@
     small = small_send(0, lambda t: TG.at[t], x, at_x)
     mark("relay")
     relays = exchange_relay()
+    drain(early)
     mark("halo2w")
     halo_finish(GC, halo)
 
@@ -577,6 +600,7 @@
 
     lax.fori_loop(0, T // R, back_body, 0)
 
+    middle = len(sent)
     mark("vg_t")
     for n in (0, 256):
         BT[n // 256, 0:256, :] = flipped(GV, n)
@@ -690,11 +714,6 @@
         BT[n // 256, 256:512, :] = flipped(GG, n)
 
     mark("partial1")
-    for cp in (gg_.h1p, gg_.h1m, gg_.d0, gg_.h2p, gg_.h2m, gg_.fp, gg_.fm, gg_.d1p, gg_.d1m,
-               gg_.d2p, gg_.d2m, gg_.d3p, gg_.d3m):
-        cp.wait_send()
-        done.append(id(cp))
-
     def partial(parity):
         def body(i, _):
             yy = i // 2
@@ -754,6 +773,7 @@
         sc[0][h].s2d()
     for cp in relays:
         cp.wait_recv()
+    drain(middle)
     mark("v_near")
     for h in (0, 1):
         spread[0][h].second()
@@ -835,13 +855,11 @@
     for h in (0, 1):
         sc[0][h].finish()
     mark("sends")
-    for cp in sent:
-        if id(cp) not in done:
-            cp.wait_send()
+    drain(len(sent))
     for d in (1, 2, 3):
         ex_b(d, (z + d) % 4).wait_send()
     mark(None)
-    assert counter[0] <= N_COPIES, counter[0]
+    assert counter[0] == N_COPIES
 
 
 def unpack(gi_in, w_in, small_in, gi, gvw, ggw, gow, gt, gg, b_out, so):
@@ -869,7 +887,7 @@
             vm((3, 256, C), BF16),
             vm((32, C), F32),
         ),
-        in_specs=[anyspace] * 5 + [in_vmem] * 2,
+        in_specs=[anyspace] * 7,
         out_specs=(in_vmem,) * 3,
         scratch_shapes=[
             vm((NB, T, C), BF16), vm((NB, T, C), BF16),
@@ -880,7 +898,7 @@
             vm((512, T), BF16), vm((2, 512, T), BF16),
             vm((T, 128), F32), vm((T, 128), F32), vm((T, 128), F32), vm((T, 128), F32),
             vm((32, C), F32),
-            vm((2, 8, T), F32), vm((2, NB, 8, T), F32),
+            vm((2, 8, 128), F32), vm((2, NB, 8, 128), F32),
             vm((32, C), F32), vm((8, C), F32),
             vm((4, 32, 128), BF16), vm((2, 32, 128), BF16), vm((3, 4, 32, 128), BF16),
             vm((1, 2, 4, 4, 256, 256), BF16),
@@ -894,9 +912,10 @@
             vm((2, 2, 2, 128, 256), BF16), vm((2, 2, 512, 256), BF16),
             vm((4, T, C), BF16),
             vm((2, 256, C), BF16), vm((2, T, C), BF16),
+            vm((TAPS, C), BF16), vm((1, C), F32),
+            pltpu.SemaphoreType.DMA((N_SENDS,)),
             pltpu.SemaphoreType.DMA((N_COPIES,)),
-            pltpu.SemaphoreType.DMA((N_COPIES,)),
-            pltpu.SemaphoreType.DMA((5,)),
+            pltpu.SemaphoreType.DMA((7,)),
         ],
         compiler_params=pltpu.CompilerParams(
             collective_id=0, has_side_effects=True, vmem_limit_bytes=64 * 1024 * 1024 - 3 * 1024 * 1024

time: 111 us -> 107 us (0.964)
  Pallas kernels: 110 us -> 106 us
    pallas_call x1, Pallas kernels: 108 us -> 104 us  [local(): pl.pallas_call(kernel, out_shape=(vm((T, C), BF16), vm((3, 256, C), BF16)...]
where the time goes in v5:
time: 107 us
  Pallas kernels  106 us (99%)
    pallas_call x1, Pallas kernels, local(): pl.pallas_call(kernel, out_shape=(vm((T, C), BF16), vm((3, 256, C), BF16)...  104 us

profile of v5, /device:TPU:1, one launch (start us, length us, event | category | flops | bytes accessed | tf_op | source)
XLA Modules:
  0.0 106.9 jit_solution(5567940132403953982)
XLA Ops:
  0.6 104.1 %shard_map.118 = (bf16[512,512]{1,0:T(8,128)(2,1)S(1)}, bf16[3,256,512]{2,1,0:T(8,128)(2,1)S(1)}, f32[32,512]{1,0:T(8,128)S(1)}) custom-call(bf16[512,512]{1,0:T(8,128)(2,1)} %x_hbm.1, bf16[512,512]{1,0:T(8,128)(2,1)} %g_hbm.1, bf16[8,512,512]{2,1,0:T(8,128)(2,1)} %bitcast.5, bf16[8,512,512]{2,1,0:T(8,128)(2,1)} %bitcast.6, bf16[8,512,512]{2,1,0:T(8,128)(2,1)} %bitcast.7, ...), custom_call_target="tpu_custom_call" | custom-call | tf_op jit(solution)/shard_map/pallas_call | solution.py:883
  104.7 2.0 %shard_map.119 = (bf16[512,512]{1,0:T(8,128)(2,1)}, f32[256,512]{1,0:T(8,128)}, f32[256,512]{1,0:T(8,128)}, f32[256,512]{1,0:T(8,128)}, f32[31,512]{1,0:T(8,128)}, /*index=5*/f32[1,512]{1,0:T(1,128)}) custom-call(bf16[512,512]{1,0:T(8,128)(2,1)S(1)} %get-tuple-element.15.gi_in, bf16[3,256,512]{2,1,0:T(8,128)(2,1)S(1)} %get-tuple-element.16.w_in, ...), custom_call_target="tpu_custom_call" | custom-call | tf_op jit(solution)/shard_map/pallas_call | solution.py:927

commit v6 on v5

--- a/solution.py
+++ b/solution.py
@@ -730,11 +730,17 @@
 
     partial(1 - c)
     swap = rcopy(G.at[pl.ds((1 - c) * 4, 4)], PR, partner)
+    mark("small")
+    TG1[0] = small_sum(0, small)
+    small = small_send(1, lambda t: TG1.at[0], z, at_z)
     mark("v_first")
     for h in (0, 1):
         spread[0][h].first()
     for h in (0, 1):
         spread[1][h].start()
+    mark("ow_s2d")
+    for h in (0, 1):
+        sc[0][h].s2d()
     mark("partial2")
     partial(c)
     mark("yadd")
@@ -762,19 +768,16 @@
     yd = rcopy(G.at[base + ym_, LO], y2.at[1, LO], at_y(y + 3))
     y_add(base + y, 0, T, [(PR, (y,), 0)])
 
+    mark("small2")
+    TG1[1] = small_sum(1, small)
+    small = small_send(2, lambda t: TG1.at[1], x, at_x)
     mark("vg_own")
     for h in (0, 1):
         vg_own(h)
-    mark("g_first")
-    for h in (0, 1):
-        spread[1][h].first()
-    mark("ow_s2d")
-    for h in (0, 1):
-        sc[0][h].s2d()
+    mark("v_near")
     for cp in relays:
         cp.wait_recv()
     drain(middle)
-    mark("v_near")
     for h in (0, 1):
         spread[0][h].second()
     for h in (0, 1):
@@ -789,6 +792,9 @@
     for dq in (1, 3, 0):
         for h in (0, 1):
             last[0][h].make(dq)
+    mark("g_first")
+    for h in (0, 1):
+        spread[1][h].first()
     mark("y_s2")
     ya.wait_recv()
     y_add(base + yp_, 0, 256, [(y1, (0,), 0)])
@@ -796,15 +802,18 @@
     yb.wait_recv()
     y_add(base + ym_, 256, 256, [(y1, (1,), 0)])
     yf = rcopy(G.at[base + ym_, HIH], y2.at[1, HIH], at_y(y + 3))
-    mark("small")
-    TG1[0] = small_sum(0, small)
-    small = small_send(1, lambda t: TG1.at[0], z, at_z)
     mark("g_second")
     for h in (0, 1):
         spread[1][h].second()
     mark("g_near")
     for h in (0, 1):
         vg_near(h, 1)
+    mark("ow_p1")
+    for h in (0, 1):
+        sc[0][h].p1()
+    mark("v_s2")
+    for h in (0, 1):
+        last[0][h].s2()
     mark("g_third")
     for h in (0, 1):
         spread[1][h].third()
@@ -812,23 +821,17 @@
     for h in (0, 1):
         last[1][h].make(2)
         last[1][h].s1()
+    mark("ow_p2")
+    for h in (0, 1):
+        sc[0][h].p2()
+    mark("g_rest")
     for dq in (1, 3, 0):
         for h in (0, 1):
             last[1][h].make(dq)
-    mark("ow_p1")
-    for h in (0, 1):
-        sc[0][h].p1()
-    TG1[1] = small_sum(1, small)
-    small = small_send(2, lambda t: TG1.at[1], x, at_x)
-    mark("v_s2")
-    for h in (0, 1):
-        last[0][h].s2()
     mark("g_s2")
     for h in (0, 1):
         last[1][h].s2()
-    mark("ow_p2")
-    for h in (0, 1):
-        sc[0][h].p2()
+    mark("small3")
     for cp in small:
         cp.wait_recv()
     for t in range(4):
@@ -845,15 +848,15 @@
         return 0
 
     lax.fori_loop(0, T // 32, gi_body, 0)
-    mark("fin")
+    mark("fin_v")
     for h in (0, 1):
         last[0][h].finish()
-    mark("g_fin")
+    mark("fin_o")
+    for h in (0, 1):
+        sc[0][h].finish()
+    mark("fin_g")
     for h in (0, 1):
         last[1][h].finish()
-    mark("ow_fin")
-    for h in (0, 1):
-        sc[0][h].finish()
     mark("sends")
     drain(len(sent))
     for d in (1, 2, 3):

time: 107 us -> 107 us (level)
  no operation moved by 1% of the time
where the time goes in v6:
time: 107 us
  Pallas kernels  106 us (99%)
    pallas_call x1, Pallas kernels, local(): pl.pallas_call(kernel, out_shape=(vm((T, C), BF16), vm((3, 256, C), BF16)...  104 us

profile of v6, /device:TPU:1, one launch (start us, length us, event | category | flops | bytes accessed | tf_op | source)
XLA Modules:
  0.0 106.8 jit_solution(2585333136751201696)
XLA Ops:
  0.6 104.0 %shard_map.118 = (bf16[512,512]{1,0:T(8,128)(2,1)S(1)}, bf16[3,256,512]{2,1,0:T(8,128)(2,1)S(1)}, f32[32,512]{1,0:T(8,128)S(1)}) custom-call(bf16[512,512]{1,0:T(8,128)(2,1)} %x_hbm.1, bf16[512,512]{1,0:T(8,128)(2,1)} %g_hbm.1, bf16[8,512,512]{2,1,0:T(8,128)(2,1)} %bitcast.5, bf16[8,512,512]{2,1,0:T(8,128)(2,1)} %bitcast.6, bf16[8,512,512]{2,1,0:T(8,128)(2,1)} %bitcast.7, ...), custom_call_target="tpu_custom_call" | custom-call | tf_op jit(solution)/shard_map/pallas_call | solution.py:886
  104.7 2.0 %shard_map.119 = (bf16[512,512]{1,0:T(8,128)(2,1)}, f32[256,512]{1,0:T(8,128)}, f32[256,512]{1,0:T(8,128)}, f32[256,512]{1,0:T(8,128)}, f32[31,512]{1,0:T(8,128)}, /*index=5*/f32[1,512]{1,0:T(1,128)}) custom-call(bf16[512,512]{1,0:T(8,128)(2,1)S(1)} %get-tuple-element.15.gi_in, bf16[3,256,512]{2,1,0:T(8,128)(2,1)S(1)} %get-tuple-element.16.w_in, ...), custom_call_target="tpu_custom_call" | custom-call | tf_op jit(solution)/shard_map/pallas_call | solution.py:930

commit v7 on v6

--- a/solution.py
+++ b/solution.py
@@ -16,8 +16,8 @@
 TAPS = 31
 PAD = 16
 COLS = (0, 128, 256, 384)
-N_COPIES = 141
-N_SENDS = 76
+N_COPIES = 108
+N_SENDS = 64
 
 
 def sig(v):
@@ -75,9 +75,18 @@
     free = list(range(N_SENDS))
     sent = []
 
-    def rcopy(src, dst, dev):
-        i = counter[0]
+    def new_recv():
         counter[0] += 1
+        return counter[0] - 1
+
+    def wait_all(ref, i):
+        pltpu.make_async_remote_copy(
+            src_ref=ref, dst_ref=ref, send_sem=ss.at[0], recv_sem=rs.at[i],
+            device_id=partner, device_id_type=MESH,
+        ).wait_recv()
+
+    def rcopy(src, dst, dev, recv=None):
+        i = new_recv() if recv is None else recv
         k = free.pop(0)
         cp = pltpu.make_async_remote_copy(
             src_ref=src, dst_ref=dst, send_sem=ss.at[k], recv_sem=rs.at[i],
@@ -91,6 +100,7 @@
         for cp, k in sent[:count]:
             cp.wait_send()
             free.append(k)
+        free.sort()
         del sent[:count]
 
     mark("entry")
@@ -171,7 +181,7 @@
         lax.fori_loop(lo, hi, body, 0)
 
     toks = pl.ds(pl.multiple_of(c * 256, 256), 256)
-    ex_a = []
+    ex_a = [None] + [new_recv() for _ in range(3)]
     b0 = counter[0]
     counter[0] += 3
     bs = free[:3]
@@ -190,7 +200,7 @@
         for d in (1, 3, 2):
             t = (x + d) % 4
             cols = pl.ds(pl.multiple_of((t % 2) * 256, 256), 256)
-            ex_a.append((d, rcopy(X.at[yy * 2 + t // 2, toks, cols], XA.at[d - 1, yy, toks], at_x(t))))
+            rcopy(X.at[yy * 2 + t // 2, toks, cols], XA.at[d - 1, yy, toks], at_x(t), ex_a[d])
 
         @pl.when(yy != z)
         def _():
@@ -199,9 +209,7 @@
     def exchange_relay():
         out = []
         for d in (1, 3, 2):
-            for dd, cp in ex_a:
-                if dd == d:
-                    cp.wait_recv()
+            wait_all(XA.at[d - 1, :, toks], ex_a[d])
             out.append(rcopy(XA.at[d - 1, :, toks], XA.at[d - 1, :, toks], partner))
         for d in (1, 3, 2):
             ex_b(d, y).wait_recv()
@@ -247,6 +255,7 @@
     gx.d3m.wait_recv()
     mm(X, vg, 2, 2, 0, 256, 2, 4)
 
+    first_sends = len(sent)
     mark("hidden")
     loads[5].wait()
     loads[6].wait()
@@ -337,11 +346,13 @@
         tile = packed
         ST[e] = tile
         STR[e, tp] = tile
-        return [rcopy(ST.at[e], STR.at[e, tp], at_tp((tp + d) % 8)) for d in range(1, 8)]
-
-    def stats_finish(e, copies):
-        for cp in copies:
-            cp.wait_recv()
+        i = new_recv()
+        for d in range(1, 8):
+            rcopy(ST.at[e], STR.at[e, tp], at_tp((tp + d) % 8), i)
+        return i
+
+    def stats_finish(e, i):
+        wait_all(STR.at[e, pl.ds(0, 7)], i)
         row = lax.broadcasted_iota(jnp.int32, (64, 256), 0) & 7
         lane = lax.broadcasted_iota(jnp.int32, (64, 256), 1)
         want = jnp.where(lane < 128, 0, 4)
@@ -367,6 +378,7 @@
     gg_.d1m.wait_recv()
     mm(G, wo, 3, 1, 0, 256, 2, 4)
     mark("g2w")
+    drain(first_sends)
     gg_.second()
     mark("g2")
     mm(G, wo, 3, 1, 256, 0, 0, 2)
@@ -494,15 +506,15 @@
             up, down = (q + 1) % 4, (q + 3) % 4
             self.i.wait_recv()
             lax.fori_loop(0, 4, self.add((p, up), 0, [(r3, (u, h, 0), 0)]), 0)
-            self.k = rcopy(part.at[u, h, p, up], r4.at[u, h, 0], at_q[h](q + 1))
+            self.k = new_recv()
+            rcopy(part.at[u, h, p, up], r4.at[u, h, 0], at_q[h](q + 1), self.k)
             self.j.wait_recv()
             lax.fori_loop(0, 4, self.add((p, down), 128, [(r3, (u, h, 1), 0)]), 0)
-            self.l = rcopy(part.at[u, h, p, down], r4.at[u, h, 1], at_q[h](q + 3))
+            rcopy(part.at[u, h, p, down], r4.at[u, h, 1], at_q[h](q + 3), self.k)
 
         def finish(self):
             u, h, p, q = self.u, self.h, self.p, self.q
-            self.k.wait_recv()
-            self.l.wait_recv()
+            wait_all(r4.at[u, h], self.k)
             for i in (0, 128):
                 rr = slice(i, i + 128)
                 v = (
@@ -566,11 +578,13 @@
 
     def small_send(e, src, me, at):
         TGR[e, me] = src(me)[...]
-        return [rcopy(src((me + d) % 4), TGR.at[e, me], at(me + d)) for d in (1, 3, 2)]
-
-    def small_sum(e, copies):
-        for cp in copies:
-            cp.wait_recv()
+        i = new_recv()
+        for d in (1, 3, 2):
+            rcopy(src((me + d) % 4), TGR.at[e, me], at(me + d), i)
+        return i
+
+    def small_sum(e, i):
+        wait_all(TGR.at[e, pl.ds(0, 3)], i)
         v = TGR[e, 0].astype(F32)
         for i in range(1, 4):
             v = v + TGR[e, i].astype(F32)
@@ -692,15 +706,15 @@
             up, down = (q + 1) % 4, (q + 3) % 4
             self.i.wait_recv()
             add(up, u * 256, 0)
-            self.k = rcopy(VP.at[h, up, rows], r4v.at[h, 0, rows], at_q[h](q + 1))
+            self.k = new_recv()
+            rcopy(VP.at[h, up, rows], r4v.at[h, 0, rows], at_q[h](q + 1), self.k)
             self.j.wait_recv()
             add(down, u * 256 + 128, 1)
-            self.l = rcopy(VP.at[h, down, rows], r4v.at[h, 1, rows], at_q[h](q + 3))
+            rcopy(VP.at[h, down, rows], r4v.at[h, 1, rows], at_q[h](q + 3), self.k)
 
         def finish(self):
             h, u, q = self.h, self.u, self.q
-            self.k.wait_recv()
-            self.l.wait_recv()
+            wait_all(r4v.at[h, :, self.rows], self.k)
             for i in (0, 128):
                 rr = slice(u * 256 + i, u * 256 + i + 128)
                 v = VP[h, q, rr].astype(F32) + r4v[h, 0, rr].astype(F32) + r4v[h, 1, rr].astype(F32)
@@ -774,6 +788,7 @@
     mark("vg_own")
     for h in (0, 1):
         vg_own(h)
+    third = len(sent) - middle
     mark("v_near")
     for cp in relays:
         cp.wait_recv()
@@ -808,6 +823,7 @@
     mark("g_near")
     for h in (0, 1):
         vg_near(h, 1)
+    drain(third)
     mark("ow_p1")
     for h in (0, 1):
         sc[0][h].p1()
@@ -832,8 +848,7 @@
     for h in (0, 1):
         last[1][h].s2()
     mark("small3")
-    for cp in small:
-        cp.wait_recv()
+    wait_all(TGR.at[2, pl.ds(0, 3)], small)
     for t in range(4):
         small_out[:, t * 128:t * 128 + 128] = TGR[2, t].astype(F32)
     mark("y_fin")

time: 107 us -> 106 us (level)
  no operation moved by 1% of the time
where the time goes in v7:
time: 106 us
  Pallas kernels  106 us (100%)
    pallas_call x1, Pallas kernels, local(): pl.pallas_call(kernel, out_shape=(vm((T, C), BF16), vm((3, 256, C), BF16)...  104 us

profile of v7, /device:TPU:1, one launch (start us, length us, event | category | flops | bytes accessed | tf_op | source)
XLA Modules:
  0.0 106.3 jit_solution(14361560227966077310)
XLA Ops:
  0.6 103.5 %shard_map.118 = (bf16[512,512]{1,0:T(8,128)(2,1)S(1)}, bf16[3,256,512]{2,1,0:T(8,128)(2,1)S(1)}, f32[32,512]{1,0:T(8,128)S(1)}) custom-call(bf16[512,512]{1,0:T(8,128)(2,1)} %x_hbm.1, bf16[512,512]{1,0:T(8,128)(2,1)} %g_hbm.1, bf16[8,512,512]{2,1,0:T(8,128)(2,1)} %bitcast.5, bf16[8,512,512]{2,1,0:T(8,128)(2,1)} %bitcast.6, bf16[8,512,512]{2,1,0:T(8,128)(2,1)} %bitcast.7, ...), custom_call_target="tpu_custom_call" | custom-call | tf_op jit(solution)/shard_map/pallas_call | solution.py:901
  104.2 2.0 %shard_map.119 = (bf16[512,512]{1,0:T(8,128)(2,1)}, f32[256,512]{1,0:T(8,128)}, f32[256,512]{1,0:T(8,128)}, f32[256,512]{1,0:T(8,128)}, f32[31,512]{1,0:T(8,128)}, /*index=5*/f32[1,512]{1,0:T(1,128)}) custom-call(bf16[512,512]{1,0:T(8,128)(2,1)S(1)} %get-tuple-element.15.gi_in, bf16[3,256,512]{2,1,0:T(8,128)(2,1)S(1)} %get-tuple-element.16.w_in, ...), custom_call_target="tpu_custom_call" | custom-call | tf_op jit(solution)/shard_map/pallas_call | solution.py:945

commit v8 on v7

--- a/solution.py
+++ b/solution.py
@@ -539,7 +539,6 @@
     mark("ow_dw2")
     dw(G, [0], AT[...], x // 2, 0, 1)
     sc[0][1].s1()
-    dw(G, [0], AT[...], x // 2, 1, 4)
     mark("stats2w")
     stats_finish(1, stats)
 
@@ -555,6 +554,7 @@
 
     lax.fori_loop(0, T // 32, gc_body, 0)
     halo = halo_start(GC)
+    dw(G, [0], AT[...], x // 2, 1, 4)
     for h in (0, 1):
         sc[0][h].s2i()
 

time: 106 us -> 106 us (level)
  no operation moved by 1% of the time
where the time goes in v8:
time: 106 us
  Pallas kernels  106 us (100%)
    pallas_call x1, Pallas kernels, local(): pl.pallas_call(kernel, out_shape=(vm((T, C), BF16), vm((3, 256, C), BF16)...  104 us

profile of v8, /device:TPU:1, one launch (start us, length us, event | category | flops | bytes accessed | tf_op | source)
XLA Modules:
  0.0 106.3 jit_solution(3060779484765555351)
XLA Ops:
  0.6 103.5 %shard_map.118 = (bf16[512,512]{1,0:T(8,128)(2,1)S(1)}, bf16[3,256,512]{2,1,0:T(8,128)(2,1)S(1)}, f32[32,512]{1,0:T(8,128)S(1)}) custom-call(bf16[512,512]{1,0:T(8,128)(2,1)} %x_hbm.1, bf16[512,512]{1,0:T(8,128)(2,1)} %g_hbm.1, bf16[8,512,512]{2,1,0:T(8,128)(2,1)} %bitcast.5, bf16[8,512,512]{2,1,0:T(8,128)(2,1)} %bitcast.6, bf16[8,512,512]{2,1,0:T(8,128)(2,1)} %bitcast.7, ...), custom_call_target="tpu_custom_call" | custom-call | tf_op jit(solution)/shard_map/pallas_call | solution.py:901
  104.2 2.0 %shard_map.119 = (bf16[512,512]{1,0:T(8,128)(2,1)}, f32[256,512]{1,0:T(8,128)}, f32[256,512]{1,0:T(8,128)}, f32[256,512]{1,0:T(8,128)}, f32[31,512]{1,0:T(8,128)}, /*index=5*/f32[1,512]{1,0:T(1,128)}) custom-call(bf16[512,512]{1,0:T(8,128)(2,1)S(1)} %get-tuple-element.15.gi_in, bf16[3,256,512]{2,1,0:T(8,128)(2,1)S(1)} %get-tuple-element.16.w_in, ...), custom_call_target="tpu_custom_call" | custom-call | tf_op jit(solution)/shard_map/pallas_call | solution.py:945
